TPU v7x, 1024 devices: a whole 8x8x8 slice. The times are simulated.
1024 devices in a mesh: ep: 64 (over z, y), tp: 16 (over x, core).
Axes of the slice: x: 8, y: 8, z: 8, core: 2. Of those that a mesh axis runs over, the one named last changes fastest.
Arguments:
- tokens: bfloat16 [10752, 2048], P('ep'), may hold values from -6 to 6
- cotangent: bfloat16 [10752, 2048], P('ep'), may hold values from -6 to 6
- group_ids: int32 [10752, 1], P('ep'), may hold values from 0 to 63; in each aligned block of 168 rows (0 to 167, 168 to 335, ...) at most 4 rows name the same one
- within_ids: int32 [10752, 2], P('ep'), may hold values from 0 to 1, all different within a row
- gate_weights: bfloat16 [10752, 2], P('ep'), may hold values from 0.099609375 to 1
- w_gate: bfloat16 [128, 2048, 1024], P('ep', None, 'tp'), may hold values from -0.125 to 0.125
- w_up: bfloat16 [128, 2048, 1024], P('ep', None, 'tp'), may hold values from -0.125 to 0.125
- w_down: bfloat16 [128, 1024, 2048], P('ep', 'tp'), may hold values from -0.1875 to 0.1875
Outputs:
- tokens_grad: bfloat16 [10752, 2048], P('ep', 'tp')
- gate_grad: float32 [10752, 2], P('ep')
- w_gate_grad: bfloat16 [128, 2048, 1024], P('ep', None, 'tp')
- w_up_grad: bfloat16 [128, 2048, 1024], P('ep', None, 'tp')
- w_down_grad: bfloat16 [128, 1024, 2048], P('ep', 'tp')
Inputs may be any that keep to these rules, and one draw needn't show every extreme that they name: `group_ids`: in the rows of one device no group is chosen by more than 4 rows. `within_ids`: the two entries of a row differ.
All inputs are finite; a program needn't handle non-finite values.
Results may differ from a plain program's by a relative error of at most 0.017.
Values may be sent and summed in bfloat16 or wider, within the bound.
No kernel may reach another device: no remote copies, remote signals or barrier semaphores. Data moves between devices by JAX's collectives and lax.ppermute only.
A program may use at most 64 MiB of HBM per device.

v0:
```python
import jax
import jax.numpy as jnp
from jax import lax
from jax.sharding import PartitionSpec as P


def side_by_side(arrays, axis, split_dim, concat_dim, along):
    ends, at = ([], 0)
    for a in arrays[:-1]:
        at += a.shape[along]
        ends.append(at)
    both = jnp.concatenate(arrays, axis=along)
    return tuple(
        jnp.split(
            lax.all_to_all(both, axis, split_axis=split_dim, concat_axis=concat_dim, tiled=True),
            ends,
            axis=along,
        )
    )


def laid_out(tiles, dim):
    tiles = jnp.moveaxis(tiles, 0, dim)
    shape = tiles.shape
    return tiles.reshape(*shape[:dim], shape[dim] * shape[dim + 1], *shape[dim + 2 :])


def copy_for_each(value, axis):
    copies = jnp.broadcast_to(value, (lax.axis_size(axis), *value.shape))
    return lax.all_to_all(copies, axis, split_axis=0, concat_axis=0, tiled=True)


def collect(value, axis, dim):
    return laid_out(copy_for_each(value, axis), dim)


def sent_together(arrays, axis, dim, along):
    ends, at = ([], 0)
    for a in arrays[:-1]:
        at += a.shape[along]
        ends.append(at)
    both = jnp.concatenate(arrays, axis=along)
    return tuple(jnp.split(collect(both, axis, dim), ends, axis=along))


def in_blocks(value, dim, peers):
    before, after = (value.shape[:dim], value.shape[dim + 1 :])
    return jnp.moveaxis(value.reshape(*before, peers, -1, *after), dim, 0)


def summed_on_arrival(value, axis, dim):
    peers = lax.axis_size(axis)
    tiles = lax.all_to_all(in_blocks(value, dim, peers), axis, 0, 0, tiled=True)
    return jnp.sum(tiles.astype(jnp.float32), axis=0)


def of_everyone(value, axis):
    return copy_for_each(value, axis).sum(axis=0)


def on_device(tokens, cotangent, group_ids, within_ids, gate_weights, w_gate, w_up, w_down):
    ep_count = lax.axis_size("ep")
    tp_count = lax.axis_size("tp")
    tok_rows, feat_width = tokens.shape
    experts_here = w_gate.shape[0]
    capacity = (3 * tok_rows + 2 * ep_count - 1) // (2 * ep_count)
    slot_count = ep_count * capacity
    group_of = group_ids[:, 0]
    in_group = (group_of[:, None] == jnp.arange(ep_count, dtype=jnp.int32)[None, :]).astype(
        jnp.float32
    )
    row_index = jnp.arange(tok_rows, dtype=jnp.int32)
    tri_lower = (row_index[:, None] > row_index[None, :]).astype(jnp.float32)
    before = jnp.dot(tri_lower, in_group, precision=lax.Precision.HIGHEST)
    rank_in = jnp.sum(before * in_group, axis=1).astype(jnp.int32)
    target = group_of * capacity + rank_in
    placing = jnp.arange(slot_count, dtype=jnp.int32)[:, None] == target[None, :]
    place_b = placing.astype(jnp.bfloat16)
    local_ids = jnp.arange(experts_here, dtype=jnp.int32)
    chosen = (within_ids[:, :, None] == local_ids[None, None, :]).astype(jnp.float32)
    combine = jnp.sum(chosen * gate_weights.astype(jnp.float32)[:, :, None], axis=1).astype(
        jnp.bfloat16
    )

    def arrange(source):
        placed = jnp.dot(place_b, source, preferred_element_type=jnp.float32).astype(jnp.bfloat16)
        return placed.reshape(ep_count, capacity, source.shape[1])

    col_share = feat_width // tp_count
    col_start = lax.axis_index("tp") * col_share
    part_x = lax.dynamic_slice_in_dim(tokens, col_start, col_share, 1)
    part_dy = lax.dynamic_slice_in_dim(cotangent, col_start, col_share, 1)
    thin_x, thin_dy, moved_comb = side_by_side(
        (arrange(part_x), arrange(part_dy), arrange(combine)), "ep", 0, 0, 2
    )
    moved_x, moved_dy = sent_together((thin_x, thin_dy), "tp", 2, 0)
    slot_x = moved_x.reshape(slot_count, feat_width)
    slot_dy = moved_dy.reshape(slot_count, feat_width)
    slot_comb = moved_comb.reshape(slot_count, experts_here)
    dy_float = slot_dy.astype(jnp.float32)
    dx_total = jnp.zeros((slot_count, feat_width), jnp.float32)
    gate_parts = []
    grads_gate = []
    grads_up = []
    grads_down = []
    for expert in range(experts_here):
        pre_gate = jnp.dot(slot_x, w_gate[expert], preferred_element_type=jnp.float32)
        pre_up = jnp.dot(slot_x, w_up[expert], preferred_element_type=jnp.float32)
        sig_gate = jax.nn.sigmoid(pre_gate)
        act_b = (pre_gate * sig_gate * pre_up).astype(jnp.bfloat16)
        down_part = jnp.dot(act_b, w_down[expert], preferred_element_type=jnp.float32)
        gate_parts.append(jnp.sum(dy_float * down_part, axis=1))
        scaled = (slot_comb[:, expert : expert + 1].astype(jnp.float32) * dy_float).astype(
            jnp.bfloat16
        )
        grads_down.append(
            jnp.einsum("sf,sd->fd", act_b, scaled, preferred_element_type=jnp.float32).astype(
                jnp.bfloat16
            )
        )
        act_grad = jnp.einsum(
            "sd,fd->sf", scaled, w_down[expert], preferred_element_type=jnp.float32
        )
        gate_b = (act_grad * pre_up * sig_gate * (1.0 + pre_gate * (1.0 - sig_gate))).astype(
            jnp.bfloat16
        )
        up_b = (act_grad * pre_gate * sig_gate).astype(jnp.bfloat16)
        grads_gate.append(
            jnp.einsum("sd,sf->df", slot_x, gate_b, preferred_element_type=jnp.float32).astype(
                jnp.bfloat16
            )
        )
        grads_up.append(
            jnp.einsum("sd,sf->df", slot_x, up_b, preferred_element_type=jnp.float32).astype(
                jnp.bfloat16
            )
        )
        dx_total = dx_total + jnp.einsum(
            "sf,df->sd", gate_b, w_gate[expert], preferred_element_type=jnp.float32
        )
        dx_total = dx_total + jnp.einsum(
            "sf,df->sd", up_b, w_up[expert], preferred_element_type=jnp.float32
        )
    gate_part = jnp.stack(gate_parts, axis=1)
    dx_share = summed_on_arrival(dx_total.astype(jnp.bfloat16), "tp", 1).astype(jnp.bfloat16)
    gate_sum = of_everyone(gate_part, "tp")
    back_dx = lax.all_to_all(
        dx_share.reshape(ep_count, capacity, dx_share.shape[1]),
        "ep",
        split_axis=0,
        concat_axis=0,
        tiled=True,
    )
    back_gate = lax.all_to_all(
        gate_sum.reshape(ep_count, capacity, experts_here),
        "ep",
        split_axis=0,
        concat_axis=0,
        tiled=True,
    )
    tokens_grad = jnp.einsum(
        "st,sd->td",
        place_b,
        back_dx.reshape(slot_count, dx_share.shape[1]),
        preferred_element_type=jnp.float32,
    ).astype(jnp.bfloat16)
    dense_gate = jnp.einsum(
        "st,se->te",
        placing.astype(jnp.float32),
        back_gate.reshape(slot_count, experts_here),
        precision=lax.Precision.HIGHEST,
    )
    gate_grad = jnp.sum(chosen * dense_gate[:, None, :], axis=2)
    return (
        tokens_grad,
        gate_grad,
        jnp.stack(grads_gate),
        jnp.stack(grads_up),
        jnp.stack(grads_down),
    )


def solution(mesh):
    in_specs = (
        P("ep", None),
        P("ep", None),
        P("ep", None),
        P("ep", None),
        P("ep", None),
        P("ep", None, "tp"),
        P("ep", None, "tp"),
        P("ep", "tp", None),
    )
    out_specs = (
        P("ep", "tp"),
        P("ep", None),
        P("ep", None, "tp"),
        P("ep", None, "tp"),
        P("ep", "tp", None),
    )
    return jax.shard_map(
        on_device, mesh=mesh, in_specs=in_specs, out_specs=out_specs, check_vma=False
    )
```

profile of v0, /device:TPU:1, one launch (start us, length us, event | category | flops | bytes accessed | tf_op | source)
XLA Modules:
  0.0 192.5 jit_solution(6185837327513474413)
XLA Ops:
  0.7 0.9 fusion.12
  1.6 0.7 convert_add_fusion
  2.3 0.7 convert_element_type.106
  3.0 0.7 select_reduce_fusion.1
  4.2 1.0 convolution_convert_fusion.7
  5.3 35.8 %all_to_all.30 = bf16[64,4,258]{2,1,0:T(4,128)(2,1)S(1)} all-to-all(bf16[64,4,258]{2,1,0:T(4,128)(2,1)S(1)} %pad_maximum_fusion.3), channel_id=1, replica_groups=mesh['ep'=64,'tp'=16] {'ep'}, dimensions={0} | all-to-all | bytes 264192 | tf_op jit(solution)/shard_map/all_to_all | solution.py:15
  41.2 2.2 %broadcast_in_dim.4 = bf16[16,128,4,128]{3,2,1,0:T(4,128)(2,1)} broadcast(bf16[128,4,128]{2,1,0:T(4,128)(2,1)S(1)} %pad_maximum_fusion.4), dimensions={1,2,3} | broadcast | bytes 2228224 | tf_op jit(solution)/shard_map/broadcast_in_dim | solution.py:29
  43.4 9.5 %all-to-all-start.1 = ((bf16[16,128,4,128]{3,2,1,0:T(4,128)(2,1)}), bf16[16,128,4,128]{3,2,1,0:T(4,128)(2,1)S(1)}, u32[]{:S(2)}, u32[]{:S(2)}) async-start(bf16[16,128,4,128]{3,2,1,0:T(4,128)(2,1)} %broadcast_in_dim.4), calls=%async_computation.1 | async-start | bytes 4194304 | tf_op jit(solution)/shard_map/all_to_all | solution.py:30
  53.4 48.5 %all-to-all-done.1 = bf16[16,128,4,128]{3,2,1,0:T(4,128)(2,1)S(1)} async-done(((bf16[16,128,4,128]{3,2,1,0:T(4,128)(2,1)}), bf16[16,128,4,128]{3,2,1,0:T(4,128)(2,1)S(1)}, u32[]{:S(2)}, u32[]{:S(2)}) %all-to-all-start.1) | async-done | bytes 2097184 | tf_op jit(solution)/shard_map/all_to_all | solution.py:30
  101.9 2.4 %copy.141 = bf16[16,128,4,128]{3,0,2,1:T(8,128)(2,1)S(1)} copy(bf16[16,128,4,128]{3,2,1,0:T(4,128)(2,1)S(1)} %all-to-all-done.1) | data formatting | bytes 4194304 | tf_op jit(solution)/shard_map/all_to_all | solution.py:30
  104.3 0.4 slice_convert_fusion
  104.8 0.6 copy-done.4
  105.4 0.4 fusion.22
  105.8 0.4 fusion.26
  106.3 0.7 multiply_convert_fusion
  107.0 0.4 fusion.15
  107.5 0.4 fusion.30
  108.1 0.5 multiply_convert_fusion.2
  108.5 0.9 fusion.10
  109.4 0.5 multiply_convert_fusion.3
  109.9 0.9 fusion.9
  110.8 0.6 broadcast_in_dim.5
  111.4 4.8 %all-to-all-start.4 = ((f32[16,256,2]{1,2,0:T(2,128)}), f32[16,256,2]{1,2,0:T(2,128)S(1)}, u32[]{:S(2)}, u32[]{:S(2)}) async-start(f32[16,256,2]{1,2,0:T(2,128)} %broadcast_in_dim.5), calls=%async_computation.4 | async-start | bytes 65536 | tf_op jit(solution)/shard_map/all_to_all | solution.py:30
  116.2 0.4 fusion.41
  116.7 0.6 copy-done.6
  117.3 0.5 convolution_add_fusion.2
  117.7 1.8 convolution_add_fusion.1
  119.5 4.1 %all-to-all-done.4 = f32[16,256,2]{1,2,0:T(2,128)S(1)} async-done(((f32[16,256,2]{1,2,0:T(2,128)}), f32[16,256,2]{1,2,0:T(2,128)S(1)}, u32[]{:S(2)}, u32[]{:S(2)}) %all-to-all-start.4) | async-done | bytes 32800 | tf_op jit(solution)/shard_map/all_to_all | solution.py:30
  123.8 0.7 copy.74
  124.4 4.8 %all-to-all-start.5 = ((f32[64,4,2]{1,2,0:T(2,128)}), f32[64,4,2]{1,2,0:T(2,128)S(1)}, u32[]{:S(2)}, u32[]{:S(2)}) async-start(f32[64,4,2]{1,2,0:T(2,128)} %copy.74), calls=%async_computation.5 | async-start | bytes 131072 | tf_op jit(solution)/shard_map/all_to_all | solution.py:154
  129.3 2.1 %fusion.11 = bf16[32,16,8,128]{3,2,1,0:T(8,128)(2,1)S(1)} fusion(f32[256,2048]{1,0:T(8,128)} %convolution_add_fusion.1, bf16[256,64]{0,1:T(8,128)(2,1)S(1)} %get-tuple-element.16, bf16[2,2048,64]{1,2,0:T(8,128)(2,1)} %param.14), kind=kOutput, calls=%fused_computation.27 | convolution fusion | flops 68157440 | bytes 3440640 | tf_op jit(solution)/shard_map/sf,df->sd/dot_general | solution.py:141
  131.4 1.3 copy.142
  132.7 7.4 %all-to-all-done.5 = f32[64,4,2]{1,2,0:T(2,128)S(1)} async-done(((f32[64,4,2]{1,2,0:T(2,128)}), f32[64,4,2]{1,2,0:T(2,128)S(1)}, u32[]{:S(2)}, u32[]{:S(2)}) %all-to-all-start.5) | async-done | bytes 2080 | tf_op jit(solution)/shard_map/all_to_all | solution.py:154
  140.2 5.6 %all-to-all-start.2 = ((bf16[16,256,128]{2,1,0:T(8,128)(2,1)}), bf16[16,256,128]{2,1,0:T(8,128)(2,1)}, u32[]{:S(2)}, u32[]{:S(2)}) async-start(bf16[16,256,128]{2,1,0:T(8,128)(2,1)} %bitcast.151), calls=%async_computation.2 | async-start | bytes 2097152 | tf_op jit(solution)/shard_map/all_to_all | solution.py:53
  145.8 1.6 fusion.3
  147.4 1.5 fusion.5
  148.9 0.3 fusion.4
  149.5 0.7 fusion.1
  150.3 0.7 fusion.2
  151.0 0.8 pad_maximum_fusion.2
  151.9 0.8 pad_maximum_fusion.1
  152.7 0.8 pad_maximum_fusion
  153.7 20.2 %all-to-all-done.2 = bf16[16,256,128]{2,1,0:T(8,128)(2,1)} async-done(((bf16[16,256,128]{2,1,0:T(8,128)(2,1)}), bf16[16,256,128]{2,1,0:T(8,128)(2,1)}, u32[]{:S(2)}, u32[]{:S(2)}) %all-to-all-start.2) | async-done | bytes 1048608 | tf_op jit(solution)/shard_map/all_to_all | solution.py:53
  173.9 2.0 %reduce_sum.68 = bf16[256,128]{1,0:T(8,128)(2,1)} reduce(bf16[16,256,128]{2,1,0:T(8,128)(2,1)} %all-to-all-done.2, bf16[]{:T(256)} %constant.20.clone.1), dimensions={0}, to_apply=%region_2.0 | reduce | flops 491520 | bytes 1114114 | tf_op jit(solution)/shard_map/reduce_sum | solution.py:54
  175.9 4.6 %all-to-all-start.3 = ((bf16[64,4,128]{2,1,0:T(4,128)(2,1)}), bf16[64,4,128]{2,1,0:T(4,128)(2,1)S(1)}, u32[]{:S(2)}, u32[]{:S(2)}) async-start(bf16[64,4,128]{2,1,0:T(4,128)(2,1)} %bitcast.13), calls=%async_computation.3 | async-start | bytes 131072 | tf_op jit(solution)/shard_map/all_to_all | solution.py:147
  180.7 0.6 select_reduce_fusion
  181.3 10.3 %all-to-all-done.3 = bf16[64,4,128]{2,1,0:T(4,128)(2,1)S(1)} async-done(((bf16[64,4,128]{2,1,0:T(4,128)(2,1)}), bf16[64,4,128]{2,1,0:T(4,128)(2,1)S(1)}, u32[]{:S(2)}, u32[]{:S(2)}) %all-to-all-start.3) | async-done | bytes 65568 | tf_op jit(solution)/shard_map/all_to_all | solution.py:147
  191.6 0.8 convolution_convert_fusion.8
  (36 shorter events, 2.2 us)
Async XLA Ops:
  0.6 3.4 %copy-start = (bf16[168,2048]{1,0:T(8,128)(2,1)S(1)}, bf16[168,2048]{1,0:T(8,128)(2,1)}, u32[]{:S(2)}) copy-start(bf16[168,2048]{1,0:T(8,128)(2,1)} %param.9) | copy-start | bytes 2064388
  43.4 58.5 %all-to-all-start.1 = ((bf16[16,128,4,128]{3,2,1,0:T(4,128)(2,1)}), bf16[16,128,4,128]{3,2,1,0:T(4,128)(2,1)S(1)}, u32[]{:S(2)}, u32[]{:S(2)}) async-start(bf16[16,128,4,128]{3,2,1,0:T(4,128)(2,1)} %broadcast_in_dim.4), calls=%async_computation.1 | async-start | bytes 4194304 | tf_op jit(solution)/shard_map/all_to_all | solution.py:30
  104.3 1.0 copy-start.4
  104.8 4.6 %copy-start.1 = (bf16[64,4,16,128]{3,2,1,0:T(8,128)(2,1)}, bf16[64,4,16,128]{3,2,1,0:T(8,128)(2,1)S(1)}, u32[]{:S(2)}) copy-start(bf16[64,4,16,128]{3,2,1,0:T(8,128)(2,1)S(1)} %get-tuple-element.6) | copy-start | bytes 3145732
  105.8 1.2 copy-start.3
  107.0 1.0 copy-start.5
  111.4 12.2 %all-to-all-start.4 = ((f32[16,256,2]{1,2,0:T(2,128)}), f32[16,256,2]{1,2,0:T(2,128)S(1)}, u32[]{:S(2)}, u32[]{:S(2)}) async-start(f32[16,256,2]{1,2,0:T(2,128)} %broadcast_in_dim.5), calls=%async_computation.4 | async-start | bytes 65536 | tf_op jit(solution)/shard_map/all_to_all | solution.py:30
  116.2 1.0 copy-start.6
  124.4 15.7 %all-to-all-start.5 = ((f32[64,4,2]{1,2,0:T(2,128)}), f32[64,4,2]{1,2,0:T(2,128)S(1)}, u32[]{:S(2)}, u32[]{:S(2)}) async-start(f32[64,4,2]{1,2,0:T(2,128)} %copy.74), calls=%async_computation.5 | async-start | bytes 131072 | tf_op jit(solution)/shard_map/all_to_all | solution.py:154
  140.2 33.8 %all-to-all-start.2 = ((bf16[16,256,128]{2,1,0:T(8,128)(2,1)}), bf16[16,256,128]{2,1,0:T(8,128)(2,1)}, u32[]{:S(2)}, u32[]{:S(2)}) async-start(bf16[16,256,128]{2,1,0:T(8,128)(2,1)} %bitcast.151), calls=%async_computation.2 | async-start | bytes 2097152 | tf_op jit(solution)/shard_map/all_to_all | solution.py:53
  145.8 3.2 %copy-start.2 = (bf16[64,4,16,128]{3,2,1,0:T(8,128)(2,1)S(1)}, bf16[64,4,16,128]{3,2,1,0:T(8,128)(2,1)}, u32[]{:S(2)}) copy-start(bf16[64,4,16,128]{3,2,1,0:T(8,128)(2,1)} %copy-done.1) | copy-start | bytes 3145732
  151.0 29.6 %copy-start.7 = (s32[168,2]{0,1:T(2,128)S(1)}, s32[168,2]{0,1:T(2,128)}, u32[]{:S(2)}) copy-start(s32[168,2]{0,1:T(2,128)} %param.11) | copy-start | bytes 4036
  175.9 15.7 %all-to-all-start.3 = ((bf16[64,4,128]{2,1,0:T(4,128)(2,1)}), bf16[64,4,128]{2,1,0:T(4,128)(2,1)S(1)}, u32[]{:S(2)}, u32[]{:S(2)}) async-start(bf16[64,4,128]{2,1,0:T(4,128)(2,1)} %bitcast.13), calls=%async_computation.3 | async-start | bytes 131072 | tf_op jit(solution)/shard_map/all_to_all | solution.py:147
where the time goes:
time: 193 us; the launch traced here: 192 us
  waiting for transfers between devices  90.5 us (47%)
  blocking collectives  35.8 us (19%)
  starting transfers between devices  29.3 us (15%)
  matrix products  17.8 us (9%)
  local copies, waits for them, and re-layouts  9.5 us (5%)
  other arithmetic  8.64 us (4%)
    all_to_all x2, waiting for transfers between devices, copy_for_each(): return lax.all_to_all(copies, axis, split_axis=0, concat_axis=0, tiled=True)  52.6 us
    all_to_all x1, blocking collectives, side_by_side(): lax.all_to_all(both, axis, split_axis=split_dim, concat_axis=concat_dim,...  35.8 us
    all_to_all x1, waiting for transfers between devices, summed_on_arrival(): tiles = lax.all_to_all(in_blocks(value, dim, peers), axis, 0, 0, tiled=True)  20.2 us
    all_to_all x2, starting transfers between devices, copy_for_each(): return lax.all_to_all(copies, axis, split_axis=0, concat_axis=0, tiled=True)  14.3 us
    all_to_all x1, waiting for transfers between devices, on_device(): lax.all_to_all(dx_share.reshape(ep_count, capacity, dx_share.shape[1]), '...  10.3 us
    all_to_all x1, waiting for transfers between devices, on_device(): lax.all_to_all(gate_sum.reshape(ep_count, capacity, experts_here), 'ep',...  7.44 us
    all_to_all x1, starting transfers between devices, summed_on_arrival(): tiles = lax.all_to_all(in_blocks(value, dim, peers), axis, 0, 0, tiled=True)  5.6 us
    all_to_all x1, starting transfers between devices, on_device(): lax.all_to_all(gate_sum.reshape(ep_count, capacity, experts_here), 'ep',...  4.8 us
  transfers between devices with their start and end apart: 5, of which 5 were waited for; matrix products, arithmetic and copies ran while one was open for 8% of the time, Pallas kernels for 0%

commit v1 on v0

v1 whole, which is shorter than its diff:
```python
import jax
import jax.numpy as jnp
from jax import lax
from jax.sharding import Mesh, PartitionSpec as P

BF16, F32, F16 = jnp.bfloat16, jnp.float32, jnp.float16
TOP = 16384.0
LEAST = 1e-30


def swap(value, axis):
    return lax.all_to_all(value, axis, split_axis=0, concat_axis=0, tiled=True)


def on_device(tokens, cotangent, group_ids, within_ids, gate_weights, w_gate, w_up, w_down):
    eps = lax.axis_size("ep")
    xs, cs = lax.axis_size("x"), lax.axis_size("c")
    tps = xs * cs
    rows, width = tokens.shape
    experts, _, hidden = w_gate.shape
    cap = (3 * rows + 2 * eps - 1) // (2 * eps)
    slots = eps * cap
    share = width // tps

    group_of = group_ids[:, 0]
    in_group = (group_of[:, None] == jnp.arange(eps, dtype=jnp.int32)[None, :]).astype(BF16)
    at = jnp.arange(rows, dtype=jnp.int32)
    earlier = (at[:, None] > at[None, :]).astype(BF16)
    before = jnp.dot(earlier, in_group, preferred_element_type=F32)
    rank = jnp.sum(before * in_group.astype(F32), axis=1).astype(jnp.int32)
    target = group_of * cap + rank
    place = (jnp.arange(slots, dtype=jnp.int32)[:, None] == target[None, :]).astype(BF16)
    local = jnp.arange(experts, dtype=jnp.int32)
    chosen = (within_ids[:, :, None] == local[None, None, :]).astype(F32)
    combine = jnp.sum(chosen * gate_weights.astype(F32)[:, :, None], axis=1).astype(BF16)
    top_x = jnp.max(jnp.abs(tokens), axis=1, keepdims=True)
    top_dy = jnp.max(jnp.abs(cotangent), axis=1, keepdims=True)

    start = (lax.axis_index("x") * cs + lax.axis_index("c")) * share
    part_x = lax.dynamic_slice_in_dim(tokens, start, share, 1)
    part_dy = lax.dynamic_slice_in_dim(cotangent, start, share, 1)
    source = jnp.concatenate([part_x, part_dy, combine, top_x, top_dy], axis=1)
    sent = jnp.dot(place, source, preferred_element_type=F32).astype(BF16)
    got = swap(sent.reshape(eps, cap, source.shape[1]), "ep").reshape(slots, source.shape[1])
    comb = got[:, 2 * share : 2 * share + experts].astype(F32)
    top = jnp.maximum(got[:, 2 * share + experts :].astype(F32), LEAST)
    up = TOP / top
    down = top * (1.0 / TOP)
    scale = jnp.repeat(up, share, axis=1)
    thin = (got[:, : 2 * share].astype(F32) * scale).astype(F16)
    full = lax.all_gather(thin, ("x", "c"))

    def whole(part, back):
        value = (part.astype(F32) * back[None]).astype(BF16)
        return jnp.moveaxis(value, 0, 1).reshape(slots, width)

    slot_x = whole(full[:, :, :share], down[:, 0:1])
    slot_dy = whole(full[:, :, share:], down[:, 1:2])

    wide = experts * hidden
    w_in = jnp.concatenate([w_gate[e] for e in range(experts)] + [w_up[e] for e in range(experts)], axis=1)
    w_out = w_down.reshape(wide, width)
    pre = jnp.dot(slot_x, w_in, preferred_element_type=F32)
    grad = jnp.einsum("sd,fd->sf", slot_dy, w_out, preferred_element_type=F32)
    pre_gate, pre_up = pre[:, :wide], pre[:, wide:]
    weight = jnp.repeat(comb, hidden, axis=1)
    sig = jax.nn.sigmoid(pre_gate)
    silu = pre_gate * sig
    act = (silu * pre_up).astype(BF16).astype(F32)
    gate_part = jnp.sum((act * grad).reshape(slots, experts, hidden), axis=2)
    act_grad = weight * grad
    gate_b = (act_grad * pre_up * sig * (1.0 + pre_gate * (1.0 - sig))).astype(BF16)
    up_b = (act_grad * silu).astype(BF16)
    both = jnp.concatenate([gate_b, up_b], axis=1)
    w_blocks = w_in.reshape(tps, share, 2 * wide)
    dx = jnp.einsum("sf,kdf->ksd", both, w_blocks, preferred_element_type=F32).astype(BF16)

    lines = slots * experts // share
    spare = -lines % 16
    gate_rows = jnp.pad(gate_part.astype(BF16).reshape(lines, share), ((0, spare), (0, 0)))
    gate_rows = jnp.broadcast_to(gate_rows, (tps, lines + spare, share))
    blocks = jnp.concatenate([dx, gate_rows], axis=1)
    tall = blocks.shape[1]
    blocks = jnp.moveaxis(blocks.reshape(xs, cs, tall, share), 1, 0)
    pair = jnp.sum(swap(blocks, "c").astype(F32), axis=0).astype(BF16)
    total = jnp.sum(swap(pair, "x").astype(F32), axis=0)
    dx_share = total[:slots].astype(BF16)
    gate_sum = total[slots : slots + lines].reshape(slots, experts)
    gate_hi = gate_sum.astype(BF16)
    gate_lo = (gate_sum - gate_hi.astype(F32)).astype(BF16)

    home = jnp.concatenate([dx_share, gate_hi, gate_lo], axis=1)
    home = swap(home.reshape(eps, cap, home.shape[1]), "ep").reshape(slots, home.shape[1])
    own = jnp.einsum("st,sd->td", place, home, preferred_element_type=F32)
    tokens_grad = own[:, :share].astype(BF16)
    dense = own[:, share : share + experts] + own[:, share + experts :]
    gate_grad = jnp.sum(chosen * dense[:, None, :], axis=2)

    w_in_grad = jnp.einsum("sd,sf->df", slot_x, both, preferred_element_type=F32).astype(BF16)
    scaled_act = (act * weight).astype(BF16)
    w_down_grad = jnp.einsum("sf,sd->fd", scaled_act, slot_dy, preferred_element_type=F32).astype(BF16)
    pieces = [w_in_grad[:, i * hidden : (i + 1) * hidden] for i in range(2 * experts)]
    return (
        tokens_grad,
        gate_grad,
        jnp.stack(pieces[:experts]),
        jnp.stack(pieces[experts:]),
        w_down_grad.reshape(experts, hidden, width),
    )


def solution(mesh):
    eps, tps = mesh.shape["ep"], mesh.shape["tp"]
    fine = Mesh(mesh.devices.reshape(eps, tps // 2, 2), ("ep", "x", "c"))
    tp = ("x", "c")
    rows = P("ep", None)
    in_specs = (rows, rows, rows, rows, rows, P("ep", None, tp), P("ep", None, tp), P("ep", tp, None))
    out_specs = (P("ep", tp), rows, P("ep", None, tp), P("ep", None, tp), P("ep", tp, None))
    return jax.shard_map(on_device, mesh=fine, in_specs=in_specs, out_specs=out_specs, check_vma=False)
```

time: 193 us -> 134 us (0.69)
  waiting for transfers between devices: 90.5 us -> 33.5 us
  matrix products: 17.8 us -> 5.74 us
  local copies, waits for them, and re-layouts: 9.5 us -> 18.8 us
  blocking collectives: 35.8 us -> 31.2 us
  starting transfers between devices: 29.3 us -> 33.7 us
    all_to_all x5 -> x3, waiting for transfers between devices: 90.5 us -> 33.5 us  [swap(): return lax.all_to_all(value, axis, split_axis=0, concat_axis=0, tiled=True)]
    all_to_all x1, blocking collectives: 35.8 us -> 5.51 us  [swap(): return lax.all_to_all(value, axis, split_axis=0, concat_axis=0, tiled=True)]
    all_gather x0 -> x1, blocking collectives: none -> 25.7 us  [on_device(): full = lax.all_gather(thin, ('x', 'c'))]
    dot_general x24 -> x8, matrix products: 17.8 us -> 5.74 us  [the longest x1 1.49 us: on_device(): jnp.einsum('sd,sf->df', slot_x, both, preferred_element_type=F32)]
    slice x1 -> x12, local copies, waits for them, and re-layouts: 0.09 us -> 6.22 us  [the longest x3 2.43 us: on_device(): w_gate[e]]
    all_to_all x5 -> x3, starting transfers between devices: 29.3 us -> 33.7 us  [swap(): return lax.all_to_all(value, axis, split_axis=0, concat_axis=0, tiled=True)]
    unnamed x18 -> x32, local copies, waits for them, and re-layouts: 1.55 us -> 5.69 us
    reduce_max x0 -> x2, other arithmetic: none -> 2.73 us  [the longest x1 1.42 us: on_device(): top_x = jnp.max(jnp.abs(tokens), axis=1, keepdims=True)]
  transfers between devices with their start and end apart: 5 -> 3, of which waited for: 5 -> 3; matrix products, arithmetic and copies ran while one was open for 8% -> 7% of each run, Pallas kernels for 0% -> 0%
where the time goes in v1:
time: 134 us; the launch traced here: 133 us
  starting transfers between devices  33.7 us (25%)
  waiting for transfers between devices  33.5 us (25%)
  blocking collectives  31.2 us (23%)
  local copies, waits for them, and re-layouts  18.8 us (14%)
  other arithmetic  9.09 us (7%)
  matrix products  5.74 us (4%)
    all_to_all x3, starting transfers between devices, swap(): return lax.all_to_all(value, axis, split_axis=0, concat_axis=0, tiled=True)  33.7 us
    all_to_all x3, waiting for transfers between devices, swap(): return lax.all_to_all(value, axis, split_axis=0, concat_axis=0, tiled=True)  33.5 us
    all_gather x1, blocking collectives, on_device(): full = lax.all_gather(thin, ('x', 'c'))  25.7 us
    unnamed x32, local copies, waits for them, and re-layouts  5.69 us
    all_to_all x1, blocking collectives, swap(): return lax.all_to_all(value, axis, split_axis=0, concat_axis=0, tiled=True)  5.51 us
  transfers between devices with their start and end apart: 3, of which 3 were waited for; matrix products, arithmetic and copies ran while one was open for 7% of the time, Pallas kernels for 0%

profile of v1, /device:TPU:1, one launch (start us, length us, event | category | flops | bytes accessed | tf_op | source)
XLA Modules:
  0.0 133.1 jit_solution(8775349242279266116)
XLA Ops:
  0.7 1.4 %abs_reduce_fusion.1 = bf16[168]{0:T(256)(128)(2,1)S(1)} fusion(bf16[168,2048]{1,0:T(8,128)(2,1)} %param.8), kind=kLoop, calls=%fused_computation.27 | loop fusion | flops 687960 | bytes 688464 | tf_op jit(solution)/shard_map/reduce_max | solution.py:36
  2.1 1.3 abs_reduce_fusion
  3.4 0.8 constant_dynamic-slice_fusion
  4.2 0.7 convert_element_type.104
  4.9 0.7 select_reduce_fusion.1
  5.9 0.9 fusion.1
  6.9 0.7 convert_add_fusion
  7.7 0.2 convolution_convert_fusion.3
  7.9 0.2 copy.128
  8.1 0.7 reshape.75
  8.8 23.9 %all-to-all-start = ((bf16[64,4,260]{2,1,0:T(4,128)(2,1)}), bf16[64,4,260]{2,1,0:T(4,128)(2,1)S(1)}, u32[]{:S(2)}, u32[]{:S(2)}) async-start(bf16[64,4,260]{2,1,0:T(4,128)(2,1)} %reshape.75), calls=%async_computation | async-start | bytes 393216 | tf_op jit(solution)/shard_map/all_to_all | solution.py:12
  32.8 1.2 fusion.32
  34.0 0.3 copy.121
  34.2 1.0 copy.122
  35.3 1.0 copy.123
  36.3 1.0 copy.124
  37.3 7.6 %all-to-all-done = bf16[64,4,260]{2,1,0:T(4,128)(2,1)S(1)} async-done(((bf16[64,4,260]{2,1,0:T(4,128)(2,1)}), bf16[64,4,260]{2,1,0:T(4,128)(2,1)S(1)}, u32[]{:S(2)}, u32[]{:S(2)}) %all-to-all-start) | async-done | bytes 133152 | tf_op jit(solution)/shard_map/all_to_all | solution.py:12
  45.0 0.3 broadcast_in_dim.13
  45.4 25.7 %all-gather.2 = f16[4096,256]{1,0:T(8,128)(2,1)S(1)} all-gather(f16[256,256]{1,0:T(8,128)(2,1)S(1)} %fusion.17), channel_id=2, replica_groups=mesh['ep'=64,'x'=8,'c'=2] {'x','c'}, dimensions={0}, use_global_device_ids=true | all-gather | bytes 2228224 | tf_op jit(solution)/shard_map/all_gather | solution.py:51
  71.1 1.6 %fusion.31 = (f16[16,256,128]{2,1,0:T(8,128)(2,1)}, f16[16,256,128]{2,1,0:T(8,128)(2,1)S(1)}) fusion(f16[16,256,256]{2,1,0:T(8,128)(2,1)S(1)} %bitcast.64), kind=kLoop, calls=%fused_computation.78 | loop fusion | bytes 4194304 | tf_op jit(solution)/shard_map/slice | solution.py:57
  72.7 2.0 %copy.150 = f16[16,256,128]{1,2,0:T(8,128)(2,1)S(1)} copy(f16[16,256,128]{2,1,0:T(8,128)(2,1)} %get-tuple-element.46) | data formatting | bytes 2097152
  74.6 0.2 slice_reduce_fusion
  74.8 1.6 %copy.149 = f16[16,256,128]{1,2,0:T(8,128)(2,1)} copy(f16[16,256,128]{2,1,0:T(8,128)(2,1)S(1)} %get-tuple-element.47) | data formatting | bytes 2097152
  76.6 0.2 multiply_convert_fusion
  76.8 1.0 copy-done.1
  77.8 0.2 multiply_convert_fusion.1
  78.0 0.4 fusion.9
  78.5 0.3 multiply_convert_fusion.4
  78.9 0.1 copy.133
  79.0 0.1 convert_element_type.122
  79.3 1.5 %convolution_convert_fusion = bf16[2048,256]{0,1:T(8,128)(2,1)} fusion(bf16[256,2048]{0,1:T(8,128)(2,1)S(1)} %bitcast.68, bf16[256,128]{0,1:T(8,128)(2,1)S(1)} %get-tuple-element.61, bf16[256,128]{0,1:T(8,128)(2,1)S(1)} %get-tuple-element.60), kind=kOutput, calls=%fused_computation | convolution fusion | flops 269221888 | bytes 2228224 | tf_op jit(solution)/shard_map/sd,sf->df/dot_general | solution.py:99
  80.9 0.8 fusion
  81.8 0.2 pad_maximum_fusion
  82.0 1.5 %copy.135 = bf16[8,2,272,128]{3,2,0,1:T(8,128)(2,1)} copy(bf16[8,2,272,128]{2,3,1,0:T(8,128)(2,1)S(1)} %bitcast.65) | data formatting | bytes 2228224 | tf_op jit(solution)/shard_map/reshape | solution.py:84
  83.6 5.5 %all_to_all.20 = bf16[2,8,272,128]{3,2,1,0:T(8,128)(2,1)S(1)} all-to-all(bf16[2,8,272,128]{3,2,1,0:T(8,128)(2,1)} %bitcast.66), channel_id=1, replica_groups=mesh['ep'=64,'x'=8,'c'=2] {'c'}, dimensions={0} | all-to-all | bytes 2228224 | tf_op jit(solution)/shard_map/all_to_all | solution.py:12
  89.1 1.1 reduce_sum.60
  90.2 5.2 %all-to-all-start.2 = ((bf16[8,272,128]{2,1,0:T(8,128)(2,1)}), bf16[8,272,128]{2,1,0:T(8,128)(2,1)S(1)}, u32[]{:S(2)}, u32[]{:S(2)}) async-start(bf16[8,272,128]{2,1,0:T(8,128)(2,1)} %reduce_sum.60), calls=%async_computation.2 | async-start | bytes 1114112 | tf_op jit(solution)/shard_map/all_to_all | solution.py:12
  95.3 1.3 slice_bitcast_fusion.1
  96.6 0.8 pad_maximum_fusion.2
  97.5 1.3 convolution_convert_fusion.1
  98.7 15.3 %all-to-all-done.2 = bf16[8,272,128]{2,1,0:T(8,128)(2,1)S(1)} async-done(((bf16[8,272,128]{2,1,0:T(8,128)(2,1)}), bf16[8,272,128]{2,1,0:T(8,128)(2,1)S(1)}, u32[]{:S(2)}, u32[]{:S(2)}) %all-to-all-start.2) | async-done | bytes 557088 | tf_op jit(solution)/shard_map/all_to_all | solution.py:12
  114.6 0.7 reshape.85
  115.3 4.6 %all-to-all-start.3 = ((bf16[64,4,132]{2,1,0:T(4,128)(2,1)}), bf16[64,4,132]{2,1,0:T(4,128)(2,1)S(1)}, u32[]{:S(2)}, u32[]{:S(2)}) async-start(bf16[64,4,132]{2,1,0:T(4,128)(2,1)} %reshape.85), calls=%async_computation.3 | async-start | bytes 262144 | tf_op jit(solution)/shard_map/all_to_all | solution.py:12
  119.9 0.8 pad_maximum_fusion.1
  120.7 10.7 %all-to-all-done.3 = bf16[64,4,132]{2,1,0:T(4,128)(2,1)S(1)} async-done(((bf16[64,4,132]{2,1,0:T(4,128)(2,1)}), bf16[64,4,132]{2,1,0:T(4,128)(2,1)S(1)}, u32[]{:S(2)}, u32[]{:S(2)}) %all-to-all-start.3) | async-done | bytes 67616 | tf_op jit(solution)/shard_map/all_to_all | solution.py:12
  131.5 0.2 fusion.18
  131.8 0.7 copy.143
  132.5 0.6 select_reduce_fusion
  (52 shorter events, 1.8 us)
Async XLA Ops:
  0.6 77.9 %copy-start = (bf16[2,64,2048]{2,1,0:T(8,128)(2,1)S(1)}, bf16[2,64,2048]{2,1,0:T(8,128)(2,1)}, u32[]{:S(2)}) copy-start(bf16[2,64,2048]{2,1,0:T(8,128)(2,1)} %param.15) | copy-start | bytes 1572868
  0.6 32.2 %copy-start.6 = (bf16[2,2048,64]{1,2,0:T(8,128)(2,1)S(1)}, bf16[2,2048,64]{1,2,0:T(8,128)(2,1)}, u32[]{:S(2)}) copy-start(bf16[2,2048,64]{1,2,0:T(8,128)(2,1)} %param.13) | copy-start | bytes 1572868
  0.7 32.2 %copy-start.7 = (bf16[2,2048,64]{1,2,0:T(8,128)(2,1)S(1)}, bf16[2,2048,64]{1,2,0:T(8,128)(2,1)}, u32[]{:S(2)}) copy-start(bf16[2,2048,64]{1,2,0:T(8,128)(2,1)} %param.14) | copy-start | bytes 1572868
  8.8 36.0 %all-to-all-start = ((bf16[64,4,260]{2,1,0:T(4,128)(2,1)}), bf16[64,4,260]{2,1,0:T(4,128)(2,1)S(1)}, u32[]{:S(2)}, u32[]{:S(2)}) async-start(bf16[64,4,260]{2,1,0:T(4,128)(2,1)} %reshape.75), calls=%async_computation | async-start | bytes 393216 | tf_op jit(solution)/shard_map/all_to_all | solution.py:12
  44.9 27.7 %copy-start.2 = (bf16[256,260]{1,0:T(8,128)(2,1)}, bf16[256,260]{1,0:T(8,128)(2,1)S(1)}, u32[]{:S(2)}) copy-start(bf16[256,260]{1,0:T(8,128)(2,1)S(1)} %reshape.76) | copy-start | bytes 399364
  72.7 3.8 %slice-start = ((bf16[256,260]{1,0:T(8,128)(2,1)}), bf16[256,2]{1,0:T(8,128)(2,1)S(1)}, s32[]{:S(2)}) async-start(bf16[256,260]{1,0:T(8,128)(2,1)} %copy-done.2), calls=%async_computation.4 | async-start | bytes 131072 | tf_op jit(solution)/shard_map/slice | solution.py:45
  76.5 1.2 copy-start.1
  76.5 1.5 %copy-start.8 = (bf16[2048,64]{0,1:T(8,128)(2,1)S(1)}, bf16[2048,64]{0,1:T(8,128)(2,1)}, u32[]{:S(2)}) copy-start(bf16[2048,64]{0,1:T(8,128)(2,1)} %get-tuple-element.53) | copy-start | bytes 786436
  76.6 1.5 %copy-start.9 = (bf16[2048,64]{0,1:T(8,128)(2,1)S(1)}, bf16[2048,64]{0,1:T(8,128)(2,1)}, u32[]{:S(2)}) copy-start(bf16[2048,64]{0,1:T(8,128)(2,1)} %get-tuple-element.54) | copy-start | bytes 786436
  76.6 1.5 %copy-start.10 = (bf16[2048,64]{0,1:T(8,128)(2,1)S(1)}, bf16[2048,64]{0,1:T(8,128)(2,1)}, u32[]{:S(2)}) copy-start(bf16[2048,64]{0,1:T(8,128)(2,1)} %get-tuple-element.70) | copy-start | bytes 786436
  76.6 1.5 %copy-start.11 = (bf16[2048,64]{0,1:T(8,128)(2,1)S(1)}, bf16[2048,64]{0,1:T(8,128)(2,1)}, u32[]{:S(2)}) copy-start(bf16[2048,64]{0,1:T(8,128)(2,1)} %get-tuple-element.71) | copy-start | bytes 786436
  79.3 1.5 %copy-start.3 = (bf16[1,2048,64]{2,1,0:T(8,128)(2,1)S(1)}, bf16[1,2048,64]{2,1,0:T(8,128)(2,1)}, u32[]{:S(2)}) copy-start(bf16[1,2048,64]{2,1,0:T(8,128)(2,1)} %copy.122) | copy-start | bytes 786436
  79.3 1.5 %copy-start.4 = (bf16[1,2048,64]{2,1,0:T(8,128)(2,1)S(1)}, bf16[1,2048,64]{2,1,0:T(8,128)(2,1)}, u32[]{:S(2)}) copy-start(bf16[1,2048,64]{2,1,0:T(8,128)(2,1)} %copy.123) | copy-start | bytes 786436
  79.3 1.5 %copy-start.5 = (bf16[1,2048,64]{2,1,0:T(8,128)(2,1)S(1)}, bf16[1,2048,64]{2,1,0:T(8,128)(2,1)}, u32[]{:S(2)}) copy-start(bf16[1,2048,64]{2,1,0:T(8,128)(2,1)} %copy.124) | copy-start | bytes 786436
  90.2 23.8 %all-to-all-start.2 = ((bf16[8,272,128]{2,1,0:T(8,128)(2,1)}), bf16[8,272,128]{2,1,0:T(8,128)(2,1)S(1)}, u32[]{:S(2)}, u32[]{:S(2)}) async-start(bf16[8,272,128]{2,1,0:T(8,128)(2,1)} %reduce_sum.60), calls=%async_computation.2 | async-start | bytes 1114112 | tf_op jit(solution)/shard_map/all_to_all | solution.py:12
  98.7 33.8 %copy-start.12 = (s32[168,2]{0,1:T(2,128)S(1)}, s32[168,2]{0,1:T(2,128)}, u32[]{:S(2)}) copy-start(s32[168,2]{0,1:T(2,128)} %param.11) | copy-start | bytes 4036
  115.3 16.2 %all-to-all-start.3 = ((bf16[64,4,132]{2,1,0:T(4,128)(2,1)}), bf16[64,4,132]{2,1,0:T(4,128)(2,1)S(1)}, u32[]{:S(2)}, u32[]{:S(2)}) async-start(bf16[64,4,132]{2,1,0:T(4,128)(2,1)} %reshape.85), calls=%async_computation.3 | async-start | bytes 262144 | tf_op jit(solution)/shard_map/all_to_all | solution.py:12

commit v2 on v1

v2 whole, which is shorter than its diff:
```python
import functools

import jax
import jax.numpy as jnp
from jax import lax
from jax.experimental import pallas as pl
from jax.experimental.pallas import tpu as pltpu
from jax.sharding import Mesh, PartitionSpec as P

BF16, F32, F16 = jnp.bfloat16, jnp.float32, jnp.float16
TILE = 8
VMEM = pl.BlockSpec(memory_space=pltpu.VMEM)
SMEM = pl.BlockSpec(memory_space=pltpu.SMEM)
ANY = pl.BlockSpec(memory_space=pl.ANY)


def swap(value, axis):
    return lax.all_to_all(value, axis, split_axis=0, concat_axis=0, tiled=True)


def dot(a, b, ca=1, cb=0):
    return lax.dot_general(a, b, (((ca,), (cb,)), ((), ())), preferred_element_type=F32)


def iota(shape, dim):
    return lax.broadcasted_iota(jnp.int32, shape, dim)


def call(body, outs, *args, flops=10**8, smem=0, scratch=(), held=(), room=20, **static):
    size = sum(a.size * a.dtype.itemsize for a in args[smem:]) + sum(o.size * o.dtype.itemsize for o in outs)
    return pl.pallas_call(
        functools.partial(body, **static) if static else body,
        out_shape=outs,
        in_specs=[SMEM if i < smem else ANY if i in held else VMEM for i in range(len(args))],
        out_specs=[VMEM] * len(outs),
        scratch_shapes=list(scratch),
        compiler_params=pltpu.CompilerParams(vmem_limit_bytes=room * 2**20),
        cost_estimate=pl.CostEstimate(flops=flops, bytes_accessed=size, transcendentals=0),
        name=body.__name__,
    )(*args)


def shape(*dims, dtype=BF16):
    return jax.ShapeDtypeStruct(dims, dtype)


def power(top):
    up, down = jnp.ones_like(top), jnp.ones_like(top)
    for k in (64, 32, 16, 8, 4, 2, 1):
        small = top < 2.0 ** (15 - k)
        step = jnp.where(small, 2.0**k, 1.0)
        top, up, down = top * step, up * step, down * jnp.where(small, 2.0**-k, 1.0)
    return up, down


def route(
    tp_ref, group_hbm, within_hbm, weight_hbm, x_hbm, dy_hbm, sent_ref, target_ref,
    group_ref, within_ref, weight_ref, x_ref, dy_ref, sems, *, eps, cap, share,
):
    pairs = (
        (group_hbm, group_ref), (within_hbm, within_ref), (weight_hbm, weight_ref), (x_hbm, x_ref), (dy_hbm, dy_ref)
    )
    copies = [pltpu.make_async_copy(hbm, ref, sems.at[i]) for i, (hbm, ref) in enumerate(pairs)]
    for copy in copies:
        copy.start()
    rows = x_ref.shape[0]
    for copy in copies[:3]:
        copy.wait()
    group = group_ref[...]
    member = iota((eps, rows), 0) == group
    earlier = (iota((rows, rows), 0) < iota((rows, rows), 1)).astype(BF16)
    before = dot(member.astype(BF16), earlier)
    rank = jnp.sum(jnp.where(member, before, 0.0), axis=0, keepdims=True).astype(jnp.int32)
    target = group * TILE + rank
    target_ref[...] = target
    row = iota((eps * TILE, rows), 0)
    place = (row == target).astype(BF16)
    beside = (row == target + cap).astype(BF16)
    within, weight = within_ref[...], weight_ref[...].astype(F32)
    expert = iota((share, rows), 0)
    combine = jnp.zeros((share, rows), F32)
    for k in range(within.shape[0]):
        combine = combine + jnp.where((expert == within[k : k + 1]) & (expert < 2), weight[k : k + 1], 0.0)
    sides = dot(beside, combine.astype(BF16), 1, 1)
    at = pl.multiple_of(tp_ref[0] * share, share)
    lane = iota((rows, share), 1)
    for copy in copies[3:]:
        copy.wait()
    parts, side = [], 0.0
    for i, ref in enumerate((x_ref, dy_ref)):
        top = jnp.max(jnp.abs(ref[...]), axis=1, keepdims=True).astype(F32)
        up, down = power(jnp.maximum(top, 2.0**-100))
        parts.append((ref[:, pl.ds(at, share)].astype(F32) * up).astype(BF16))
        side = side + jnp.where(lane == 2 + i, down, 0.0)
    sides = sides + dot(beside, side.astype(BF16))
    sent_ref[:, :share] = (dot(place, parts[0]) + sides).astype(BF16)
    sent_ref[:, share:] = dot(place, parts[1]).astype(BF16)


def split(value):
    hi = value.astype(BF16).astype(F32)
    return hi, value - hi


def four(first, second):
    a, b = split(first), split(second)
    return [a[0], b[0], a[1], b[1]]


def experts(
    c_ref, full_ref, got_ref, gate_ref, up_ref, down_ref, gate2_ref, up2_ref, down2_ref,
    out_ref, thin_ref, x_ref, dy_ref, *, cap,
):
    tps, slots, two = full_ref.shape
    share = two // 2
    wide = gate_ref.shape[0]
    for k in range(tps):
        x_ref[:, k * share : k * share + share] = full_ref[k, :, :share]
        dy_ref[:, k * share : k * share + share] = full_ref[k, :, share:]
    slot, row = iota((slots, got_ref.shape[0]), 0), iota((slots, got_ref.shape[0]), 1)
    pick = (row == slot // cap * TILE + cap + slot % cap).astype(BF16)
    side = dot(pick, got_ref[:, :share])
    back_x, back_dy = side[:, 2:3], side[:, 3:4]
    lane = iota((slots, 2 * wide), 1)
    weight = jnp.where(lane % wide < wide // 2, side[:, 0:1], side[:, 1:2])
    gates = jnp.concatenate([gate_ref[...], gate2_ref[...]], axis=0)
    ups = jnp.concatenate([up_ref[...], up2_ref[...]], axis=0)
    downs = jnp.concatenate([down_ref[...], down2_ref[...]], axis=0)
    pre_gate = dot(x_ref[...], gates, 1, 1) * back_x
    pre_up = dot(x_ref[...], ups, 1, 1) * back_x
    grad = dot(dy_ref[...], downs, 1, 1) * back_dy
    sig = jax.nn.sigmoid(pre_gate)
    silu = pre_gate * sig
    act = (silu * pre_up).astype(BF16).astype(F32)
    thin_ref[:, 2 * wide :] = (act * weight * back_dy)[:, :wide].astype(BF16)
    hi, lo = split(act * grad)
    ones = (iota((16, 2 * wide), 0) == iota((16, 2 * wide), 1) % wide // (wide // 2)).astype(BF16)
    sums = dot(ones, hi.astype(BF16), 1, 1) + dot(ones, lo.astype(BF16), 1, 1)
    lines = jnp.concatenate(four(sums[0:1], sums[1:2]), axis=0)
    lines = jnp.concatenate([lines[:, :share], lines[:, share:]], axis=0).astype(BF16)
    act_grad = weight * grad
    gate_b = (act_grad * pre_up * sig * (1.0 + pre_gate * (1.0 - sig))).astype(BF16)
    up_b = (act_grad * silu).astype(BF16)
    thin_ref[:, :wide] = (gate_b[:, :wide].astype(F32) * back_x).astype(BF16)
    thin_ref[:, wide : 2 * wide] = (up_b[:, :wide].astype(F32) * back_x).astype(BF16)
    for x in range(0, tps // 2, 2):
        at = [pl.ds(pl.multiple_of((2 * (x + i) + c_ref[0]) * share, share), share) for i in range(2)]
        dx = 0.0
        for value, refs in ((gate_b, (gate_ref, gate2_ref)), (up_b, (up_ref, up2_ref))):
            block = [jnp.concatenate([ref[:, a] for a in at], axis=1) for ref in refs]
            dx = dx + dot(value, jnp.concatenate(block, axis=0))
        for i in range(2):
            out_ref[x + i, :slots, :] = dx[:, i * share : i * share + share].astype(BF16)
            out_ref[x + i, slots:, :] = lines


def gather_up(blocks_ref, out_ref, *, cap):
    xs, tall, share = blocks_ref.shape
    slots = tall - 8
    total = blocks_ref[0].astype(F32)
    for x in range(1, xs):
        total = total + blocks_ref[x].astype(F32)
    dx = total[:slots].astype(BF16)
    lines = jnp.concatenate([total[slots : slots + 4], total[slots + 4 :]], axis=1)
    lines = four(lines[0:1] + lines[2:3], lines[1:2] + lines[3:4])
    lines = jnp.concatenate(lines + [jnp.zeros((share - 4, slots), F32)], axis=0).astype(BF16)
    row, slot = iota((out_ref.shape[0], slots), 0), iota((out_ref.shape[0], slots), 1)
    at = slot // cap * TILE + slot % cap
    out = dot((row == at).astype(BF16), dx) + dot((row == at + cap).astype(BF16), lines, 1, 1)
    out_ref[...] = out.astype(BF16)


def settle(target_ref, within_ref, home_ref, out_ref, gate_ref, *, cap):
    rows = out_ref.shape[0]
    row = iota((home_ref.shape[0], rows), 0)
    target = target_ref[...]
    home = home_ref[...]
    out_ref[...] = dot((row == target).astype(BF16), home, 0, 0).astype(BF16)
    dense = dot(home, (row == target + cap).astype(BF16), 0, 0)
    first = dense[0:1] + dense[2:3]
    second = dense[1:2] + dense[3:4]
    gate_ref[...] = jnp.where(within_ref[...] == 0, first, second)


def weights(full_ref, thin_ref, gate_ref, up_ref, down_ref):
    tps, slots, two = full_ref.shape
    share = two // 2
    wide = gate_ref.shape[0]
    for k in range(0, tps, 2):
        cols = slice(k * share, (k + 2) * share)
        x = jnp.concatenate([full_ref[k, :, :share], full_ref[k + 1, :, :share]], axis=1)
        dy = jnp.concatenate([full_ref[k, :, share:], full_ref[k + 1, :, share:]], axis=1)
        both = dot(thin_ref[:, : 2 * wide], x, 0, 0).astype(BF16)
        gate_ref[:, cols] = both[:wide]
        up_ref[:, cols] = both[wide:]
        down_ref[:, cols] = dot(thin_ref[:, 2 * wide :], dy, 0, 0).astype(BF16)


def on_device(tokens, cotangent, group_ids, within_ids, gate_weights, w_gate, w_up, w_down):
    eps = lax.axis_size("ep")
    xs, cs = lax.axis_size("x"), lax.axis_size("c")
    tps = xs * cs
    rows, width = tokens.shape
    count, _, hidden = w_gate.shape
    wide = count * hidden
    cap = (3 * rows + 2 * eps - 1) // (2 * eps)
    slots = eps * cap
    share = width // tps
    c = lax.axis_index("c").astype(jnp.int32)
    tp1 = (lax.axis_index("x").astype(jnp.int32) * cs + c).reshape(1)
    mine = (
        jnp.swapaxes(w_gate, 1, 2).reshape(wide, width),
        jnp.swapaxes(w_up, 1, 2).reshape(wide, width),
        w_down.reshape(wide, width),
    )
    within_t = within_ids.T

    sent, target = call(
        route,
        [shape(eps * TILE, 2 * share), shape(1, rows, dtype=jnp.int32)],
        tp1, group_ids.T, within_t, gate_weights.T, tokens, cotangent,
        smem=1, held=(1, 2, 3, 4, 5), room=58, eps=eps, cap=cap, share=share,
        scratch=[
            pltpu.VMEM((1, rows), jnp.int32), pltpu.VMEM((2, rows), jnp.int32), pltpu.VMEM((2, rows), BF16),
            pltpu.VMEM((rows, width), BF16), pltpu.VMEM((rows, width), BF16), pltpu.SemaphoreType.DMA((5,)),
        ],
    )
    got = swap(sent.reshape(eps, TILE, 2 * share), "ep")
    theirs = [lax.ppermute(w, "c", [(0, 1), (1, 0)]) for w in mine]
    thin = got[:, :cap, :].reshape(slots, 2 * share).astype(F16)
    full = lax.all_gather(thin, ("x", "c")).astype(BF16)

    blocks, thin_b = call(
        experts,
        [shape(xs, slots + 8, share), shape(slots, 3 * wide)],
        c.reshape(1), full, got.reshape(eps * TILE, 2 * share), *mine, *theirs,
        smem=1, flops=10**9, scratch=[pltpu.VMEM((slots, width), BF16)] * 2, cap=cap,
    )
    blocks = swap(blocks, "x")
    (home,) = call(gather_up, [shape(eps * TILE, share)], blocks, cap=cap)
    thin_b, home = lax.optimization_barrier((thin_b, home))
    home = swap(home.reshape(eps, TILE, share), "ep").reshape(eps * TILE, share)
    tokens_grad, gate_grad = call(
        settle, [shape(rows, share), shape(2, rows, dtype=F32)], target, within_t, home, cap=cap
    )
    gate_g, up_g, down_g = call(weights, [shape(wide, width)] * 3, full, thin_b, flops=10**9)
    return (
        tokens_grad,
        gate_grad.T,
        jnp.swapaxes(gate_g.reshape(count, hidden, width), 1, 2),
        jnp.swapaxes(up_g.reshape(count, hidden, width), 1, 2),
        down_g.reshape(count, hidden, width),
    )


def solution(mesh):
    eps, tps = mesh.shape["ep"], mesh.shape["tp"]
    fine = Mesh(mesh.devices.reshape(eps, tps // 2, 2), ("ep", "x", "c"))
    tp = ("x", "c")
    rows = P("ep", None)
    in_specs = (rows, rows, rows, rows, rows, P("ep", None, tp), P("ep", None, tp), P("ep", tp, None))
    out_specs = (P("ep", tp), rows, P("ep", None, tp), P("ep", None, tp), P("ep", tp, None))
    return jax.shard_map(on_device, mesh=fine, in_specs=in_specs, out_specs=out_specs, check_vma=False)
```

time: 134 us -> 114 us (0.85)
  waiting for transfers between devices: 33.5 us -> 14.5 us
  blocking collectives: 31.2 us -> 49.2 us
  local copies, waits for them, and re-layouts: 18.8 us -> 2.52 us
  Pallas kernels: 0 us -> 9.65 us
  other arithmetic: 9.09 us -> 0.5 us
  matrix products: 5.74 us -> 0 us
  starting transfers between devices: 33.7 us -> 35.9 us
    all_to_all x3 -> x2, waiting for transfers between devices: 33.5 us -> 14.5 us  [swap(): return lax.all_to_all(value, axis, split_axis=0, concat_axis=0, tiled=True)]
    all_to_all x1, blocking collectives: 5.51 us -> 23.1 us  [swap(): return lax.all_to_all(value, axis, split_axis=0, concat_axis=0, tiled=True)]
    pallas_call x0 -> x5, Pallas kernels: none -> 9.65 us  [call(): pl.pallas_call(functools.partial(body, **static) if static else body, out...]
    ppermute x0 -> x3, starting transfers between devices: none -> 7.2 us  [on_device(): theirs = [lax.ppermute(w, 'c', [(0, 1), (1, 0)]) for w in mine]]
    slice x12 -> x0, local copies, waits for them, and re-layouts: 6.22 us -> none  [the longest x3 2.43 us: on_device(): w_gate[e]]
    dot_general x8 -> x0, matrix products: 5.74 us -> none  [the longest x1 1.49 us: on_device(): jnp.einsum('sd,sf->df', slot_x, both, preferred_element_type=F32)]
    all_to_all x3 -> x2, starting transfers between devices: 33.7 us -> 28.7 us  [swap(): return lax.all_to_all(value, axis, split_axis=0, concat_axis=0, tiled=True)]
    reshape x7 -> x0, local copies, waits for them, and re-layouts: 3.34 us -> none  [the longest x1 1.54 us: on_device(): blocks = jnp.moveaxis(blocks.reshape(xs, cs, tall, share), 1, 0)]
  transfers between devices with their start and end apart: 3 -> 5, of which waited for: 3 -> 2; matrix products, arithmetic and copies ran while one was open for 7% -> 0% of each run, Pallas kernels for 0% -> 2%
where the time goes in v2:
time: 114 us; the launch traced here: 113 us
  blocking collectives  49.2 us (43%)
  starting transfers between devices  35.9 us (31%)
  waiting for transfers between devices  14.5 us (13%)
  Pallas kernels  9.65 us (8%)
  local copies, waits for them, and re-layouts  2.52 us (2%)
    all_to_all x2, starting transfers between devices, swap(): return lax.all_to_all(value, axis, split_axis=0, concat_axis=0, tiled=True)  28.7 us
    all_gather x1, blocking collectives, on_device(): full = lax.all_gather(thin, ('x', 'c')).astype(BF16)  26 us
    all_to_all x1, blocking collectives, swap(): return lax.all_to_all(value, axis, split_axis=0, concat_axis=0, tiled=True)  23.1 us
    all_to_all x2, waiting for transfers between devices, swap(): return lax.all_to_all(value, axis, split_axis=0, concat_axis=0, tiled=True)  14.5 us
    pallas_call x5, Pallas kernels, call(): pl.pallas_call(functools.partial(body, **static) if static else body, out...  9.65 us
    ppermute x3, starting transfers between devices, on_device(): theirs = [lax.ppermute(w, 'c', [(0, 1), (1, 0)]) for w in mine]  7.2 us
    unnamed x14, local copies, waits for them, and re-layouts  2.47 us
  transfers between devices with their start and end apart: 5, of which 2 were waited for; matrix products, arithmetic and copies ran while one was open for 0% of the time, Pallas kernels for 2%

profile of v2, /device:TPU:1, one launch (start us, length us, event | category | flops | bytes accessed | tf_op | source)
XLA Modules:
  0.0 113.0 jit_solution(5769285403181170623)
XLA Ops:
  0.6 2.9 %route.1 = (bf16[512,256]{1,0:T(8,128)(2,1)}, s32[1,168]{1,0:T(1,128)}) custom-call(s32[1]{0:T(128)} %bitcast.tp_ref, s32[1,168]{1,0:T(1,128)} %bitcast.35, s32[2,168]{1,0:T(2,128)} %bitcast.32, bf16[2,168]{1,0:T(2,128)(2,1)} %bitcast.36, bf16[168,2048]{1,0:T(8,128)(2,1)} %x_hbm.1, bf16[168,2048]{1,0:T(8,128)(2,1)} %dy_hbm.1), custom_call_target="tpu_custom_call" | custom-call | flops 100000000 | bytes 1641760 | tf_op jit(solution)/shard_map/route/pallas_call | solution.py:31
  3.6 24.0 %all-to-all-start = ((bf16[64,8,256]{2,1,0:T(8,128)(2,1)}), bf16[64,8,256]{2,1,0:T(8,128)(2,1)S(1)}, u32[]{:S(2)}, u32[]{:S(2)}) async-start(bf16[64,8,256]{2,1,0:T(8,128)(2,1)} %bitcast.34), calls=%async_computation | async-start | bytes 524288 | tf_op jit(solution)/shard_map/all_to_all | solution.py:18
  27.5 2.9 %collective-permute-start = (bf16[128,2048]{1,0:T(8,128)(2,1)}, bf16[128,2048]{1,0:T(8,128)(2,1)S(1)}, u32[]{:S(2)}, u32[]{:S(2)}) collective-permute-start(bf16[128,2048]{1,0:T(8,128)(2,1)} %bitcast.25), channel_id=1, source_target_pairs={{0,1},{1,0},{2,3},{3,2},{4,5},{5,4},{6,7},{7,6},{8,9},{9,8},{10,11... | collective-permute-start | bytes 1572872 | tf_op jit(solution)/shard_map/ppermute | solution.py:229
  30.4 1.9 %collective-permute-start.1 = (bf16[128,2048]{1,0:T(8,128)(2,1)}, bf16[128,2048]{1,0:T(8,128)(2,1)S(1)}, u32[]{:S(2)}, u32[]{:S(2)}) collective-permute-start(bf16[128,2048]{1,0:T(8,128)(2,1)} %bitcast.27), channel_id=1, source_target_pairs={{0,1},{1,0},{2,3},{3,2},{4,5},{5,4},{6,7},{7,6},{8,9},{9,8},{10,11... | collective-permute-start | bytes 1572872 | tf_op jit(solution)/shard_map/ppermute | solution.py:229
  32.3 2.4 %collective-permute-start.2 = (bf16[128,2048]{1,0:T(8,128)(2,1)}, bf16[128,2048]{1,0:T(8,128)(2,1)}, u32[]{:S(2)}, u32[]{:S(2)}) collective-permute-start(bf16[128,2048]{1,0:T(8,128)(2,1)} %bitcast.29), channel_id=1, source_target_pairs={{0,1},{1,0},{2,3},{3,2},{4,5},{5,4},{6,7},{7,6},{8,9},{9,8},{10,11... | collective-permute-start | bytes 1572872 | tf_op jit(solution)/shard_map/ppermute | solution.py:229
  34.7 5.6 %all-to-all-done = bf16[64,8,256]{2,1,0:T(8,128)(2,1)S(1)} async-done(((bf16[64,8,256]{2,1,0:T(8,128)(2,1)}), bf16[64,8,256]{2,1,0:T(8,128)(2,1)S(1)}, u32[]{:S(2)}, u32[]{:S(2)}) %all-to-all-start) | async-done | bytes 262176 | tf_op jit(solution)/shard_map/all_to_all | solution.py:18
  40.4 0.1 slice_convert_fusion
  40.5 26.0 %all-gather.1 = f16[16,256,256]{2,1,0:T(8,128)(2,1)S(1)} all-gather(f16[1,256,256]{2,1,0:T(8,128)(2,1)S(1)} %convert_element_type.17), channel_id=1, replica_groups=mesh['ep'=64,'x'=8,'c'=2] {'x','c'}, dimensions={0}, use_global_device_ids=true | all-gather | bytes 2228224 | tf_op jit(solution)/shard_map/all_gather | solution.py:231
  66.5 0.0 copy-start
  66.5 0.0 copy-start.1
  66.5 0.0 copy-start.2
  66.5 0.4 convert_element_type.18.full_ref
  67.0 0.0 collective-permute-done.gate2_ref
  67.0 0.0 collective-permute-done.1.up2_ref
  67.0 0.0 collective-permute-done.2.down2_ref
  67.0 0.6 copy-done
  67.6 0.2 copy-done.1
  67.7 0.2 copy-done.2
  67.9 3.2 %experts.1 = (bf16[8,264,128]{2,1,0:T(8,128)(2,1)S(1)}, bf16[256,384]{1,0:T(8,128)(2,1)S(1)}) custom-call(s32[1]{0:T(128)} %bitcast.4.c_ref, bf16[16,256,256]{2,1,0:T(8,128)(2,1)S(1)} %convert_element_type.18.full_ref, bf16[512,256]{1,0:T(8,128)(2,1)S(1)} %bitcast.24, bf16[128,2048]{1,0:T(8,128)(2,1)S(1)} %bitcast.26, bf16[128,2048]{1,0:T(8,128)(2,1)S(1)} %bitcast.28, ...), custom_call_target="tpu_custom_call" | custom-call | flops 1000000000 | bytes 6242304 | tf_op jit(solution)/shard_map/experts/pallas_call | solution.py:31
  71.0 0.0 copy-start.4
  71.1 0.7 copy-done.4
  71.7 23.1 %all_to_all.15.blocks_ref = bf16[8,264,128]{2,1,0:T(8,128)(2,1)S(1)} all-to-all(bf16[8,264,128]{2,1,0:T(8,128)(2,1)S(1)} %get-tuple-element.19), channel_id=1, replica_groups=mesh['ep'=64,'x'=8,'c'=2] {'x'}, dimensions={0} | all-to-all | bytes 1081344 | tf_op jit(solution)/shard_map/all_to_all | solution.py:18
  94.8 1.0 gather_up.1
  95.8 0.0 copy-start.3
  95.8 0.0 copy-start.6
  95.8 4.7 %all-to-all-start.2 = ((bf16[64,8,128]{2,1,0:T(8,128)(2,1)}), bf16[64,8,128]{2,1,0:T(8,128)(2,1)S(1)}, u32[]{:S(2)}, u32[]{:S(2)}) async-start(bf16[64,8,128]{2,1,0:T(8,128)(2,1)} %bitcast.14), calls=%async_computation.2 | async-start | bytes 262144 | tf_op jit(solution)/shard_map/all_to_all | solution.py:18
  100.6 0.0 copy-start.5
  100.6 0.9 copy-done.5
  101.5 1.7 %weights.1 = (bf16[128,2048]{1,0:T(8,128)(2,1)}, bf16[128,2048]{1,0:T(8,128)(2,1)}, bf16[128,2048]{1,0:T(8,128)(2,1)}) custom-call(bf16[16,256,256]{2,1,0:T(8,128)(2,1)S(1)} %convert_element_type.18.full_ref, bf16[256,384]{1,0:T(8,128)(2,1)S(1)} %copy-done.5), custom_call_target="tpu_custom_call" | custom-call | flops 1000000000 | bytes 3866624 | tf_op jit(solution)/shard_map/weights/pallas_call | solution.py:31
  103.2 8.9 %all-to-all-done.2 = bf16[64,8,128]{2,1,0:T(8,128)(2,1)S(1)} async-done(((bf16[64,8,128]{2,1,0:T(8,128)(2,1)}), bf16[64,8,128]{2,1,0:T(8,128)(2,1)S(1)}, u32[]{:S(2)}, u32[]{:S(2)}) %all-to-all-start.2) | async-done | bytes 131104 | tf_op jit(solution)/shard_map/all_to_all | solution.py:18
  112.1 0.0 copy-done.3
  112.1 0.0 copy-done.6
  112.1 0.9 settle.1
  (1 shorter events, 0.0 us)
Async XLA Ops:
  3.6 36.8 %all-to-all-start = ((bf16[64,8,256]{2,1,0:T(8,128)(2,1)}), bf16[64,8,256]{2,1,0:T(8,128)(2,1)S(1)}, u32[]{:S(2)}, u32[]{:S(2)}) async-start(bf16[64,8,256]{2,1,0:T(8,128)(2,1)} %bitcast.34), calls=%async_computation | async-start | bytes 524288 | tf_op jit(solution)/shard_map/all_to_all | solution.py:18
  27.5 39.5 %collective-permute-start = (bf16[128,2048]{1,0:T(8,128)(2,1)}, bf16[128,2048]{1,0:T(8,128)(2,1)S(1)}, u32[]{:S(2)}, u32[]{:S(2)}) collective-permute-start(bf16[128,2048]{1,0:T(8,128)(2,1)} %bitcast.25), channel_id=1, source_target_pairs={{0,1},{1,0},{2,3},{3,2},{4,5},{5,4},{6,7},{7,6},{8,9},{9,8},{10,11... | collective-permute-start | bytes 1572872 | tf_op jit(solution)/shard_map/ppermute | solution.py:229
  30.4 36.6 %collective-permute-start.1 = (bf16[128,2048]{1,0:T(8,128)(2,1)}, bf16[128,2048]{1,0:T(8,128)(2,1)S(1)}, u32[]{:S(2)}, u32[]{:S(2)}) collective-permute-start(bf16[128,2048]{1,0:T(8,128)(2,1)} %bitcast.27), channel_id=1, source_target_pairs={{0,1},{1,0},{2,3},{3,2},{4,5},{5,4},{6,7},{7,6},{8,9},{9,8},{10,11... | collective-permute-start | bytes 1572872 | tf_op jit(solution)/shard_map/ppermute | solution.py:229
  32.3 34.7 %collective-permute-start.2 = (bf16[128,2048]{1,0:T(8,128)(2,1)}, bf16[128,2048]{1,0:T(8,128)(2,1)}, u32[]{:S(2)}, u32[]{:S(2)}) collective-permute-start(bf16[128,2048]{1,0:T(8,128)(2,1)} %bitcast.29), channel_id=1, source_target_pairs={{0,1},{1,0},{2,3},{3,2},{4,5},{5,4},{6,7},{7,6},{8,9},{9,8},{10,11... | collective-permute-start | bytes 1572872 | tf_op jit(solution)/shard_map/ppermute | solution.py:229
  66.5 1.0 copy-start
  66.5 1.2 %copy-start.1 = (bf16[2,2048,64]{1,2,0:T(8,128)(2,1)S(1)}, bf16[2,2048,64]{1,2,0:T(8,128)(2,1)}, u32[]{:S(2)}) copy-start(bf16[2,2048,64]{1,2,0:T(8,128)(2,1)} %param.14) | copy-start | bytes 1572868
  66.5 1.4 %copy-start.2 = (bf16[2,64,2048]{2,1,0:T(8,128)(2,1)S(1)}, bf16[2,64,2048]{2,1,0:T(8,128)(2,1)}, u32[]{:S(2)}) copy-start(bf16[2,64,2048]{2,1,0:T(8,128)(2,1)} %param.15) | copy-start | bytes 1572868
  71.0 0.7 copy-start.4
  95.8 16.3 %copy-start.3 = (s32[168,2]{0,1:T(2,128)S(1)}, s32[168,2]{0,1:T(2,128)}, u32[]{:S(2)}) copy-start(s32[168,2]{0,1:T(2,128)} %param.11) | copy-start | bytes 4036
  95.8 16.3 %copy-start.6 = (s32[1,168]{1,0:T(1,128)S(1)}, s32[1,168]{1,0:T(1,128)}, u32[]{:S(2)}) copy-start(s32[1,168]{1,0:T(1,128)} %get-tuple-element.16.target_ref) | copy-start | bytes 2020
  95.8 16.3 %all-to-all-start.2 = ((bf16[64,8,128]{2,1,0:T(8,128)(2,1)}), bf16[64,8,128]{2,1,0:T(8,128)(2,1)S(1)}, u32[]{:S(2)}, u32[]{:S(2)}) async-start(bf16[64,8,128]{2,1,0:T(8,128)(2,1)} %bitcast.14), calls=%async_computation.2 | async-start | bytes 262144 | tf_op jit(solution)/shard_map/all_to_all | solution.py:18
  100.6 0.9 copy-start.5

commit v3 on v2

--- a/solution.py
+++ b/solution.py
@@ -108,47 +108,52 @@
 
 
 def experts(
-    c_ref, full_ref, got_ref, gate_ref, up_ref, down_ref, gate2_ref, up2_ref, down2_ref,
-    out_ref, thin_ref, x_ref, dy_ref, *, cap,
+    c_ref, full_ref, got_ref, mine_hbm, theirs_hbm, out_ref, thin_ref, x_ref, dy_ref, in_ref, down_ref, sems, *, cap
 ):
     tps, slots, two = full_ref.shape
     share = two // 2
-    wide = gate_ref.shape[0]
+    wide = down_ref.shape[0] // 2
+    piece = wide // 2
+    copies = []
+    for i, hbm in enumerate((mine_hbm, theirs_hbm)):
+        for j in range(6):
+            ref, at = (in_ref, 2 * wide * i + piece * j) if j < 4 else (down_ref, wide * i + piece * (j - 4))
+            copies.append(
+                pltpu.make_async_copy(hbm.at[pl.ds(piece * j, piece)], ref.at[pl.ds(at, piece)], sems.at[i, j])
+            )
+            copies[-1].start()
     for k in range(tps):
         x_ref[:, k * share : k * share + share] = full_ref[k, :, :share]
         dy_ref[:, k * share : k * share + share] = full_ref[k, :, share:]
     slot, row = iota((slots, got_ref.shape[0]), 0), iota((slots, got_ref.shape[0]), 1)
     pick = (row == slot // cap * TILE + cap + slot % cap).astype(BF16)
     side = dot(pick, got_ref[:, :share])
+    for copy in copies:
+        copy.wait()
     back_x, back_dy = side[:, 2:3], side[:, 3:4]
     lane = iota((slots, 2 * wide), 1)
     weight = jnp.where(lane % wide < wide // 2, side[:, 0:1], side[:, 1:2])
-    gates = jnp.concatenate([gate_ref[...], gate2_ref[...]], axis=0)
-    ups = jnp.concatenate([up_ref[...], up2_ref[...]], axis=0)
-    downs = jnp.concatenate([down_ref[...], down2_ref[...]], axis=0)
-    pre_gate = dot(x_ref[...], gates, 1, 1) * back_x
-    pre_up = dot(x_ref[...], ups, 1, 1) * back_x
-    grad = dot(dy_ref[...], downs, 1, 1) * back_dy
+    pre = dot(x_ref[...], in_ref[...], 1, 1) * back_x
+    grad = dot(dy_ref[...], down_ref[...], 1, 1) * back_dy
+    pre_gate = jnp.concatenate([pre[:, :wide], pre[:, 2 * wide : 3 * wide]], axis=1)
+    pre_up = jnp.concatenate([pre[:, wide : 2 * wide], pre[:, 3 * wide :]], axis=1)
     sig = jax.nn.sigmoid(pre_gate)
     silu = pre_gate * sig
     act = (silu * pre_up).astype(BF16).astype(F32)
+    act_grad = weight * grad
+    gate_b = (act_grad * pre_up * sig * (1.0 + pre_gate * (1.0 - sig))).astype(BF16)
+    up_b = (act_grad * silu).astype(BF16)
+    both = jnp.concatenate([gate_b[:, :wide], up_b[:, :wide], gate_b[:, wide:], up_b[:, wide:]], axis=1)
+    thin_ref[:, : 2 * wide] = (both[:, : 2 * wide].astype(F32) * back_x).astype(BF16)
     thin_ref[:, 2 * wide :] = (act * weight * back_dy)[:, :wide].astype(BF16)
     hi, lo = split(act * grad)
     ones = (iota((16, 2 * wide), 0) == iota((16, 2 * wide), 1) % wide // (wide // 2)).astype(BF16)
     sums = dot(ones, hi.astype(BF16), 1, 1) + dot(ones, lo.astype(BF16), 1, 1)
     lines = jnp.concatenate(four(sums[0:1], sums[1:2]), axis=0)
     lines = jnp.concatenate([lines[:, :share], lines[:, share:]], axis=0).astype(BF16)
-    act_grad = weight * grad
-    gate_b = (act_grad * pre_up * sig * (1.0 + pre_gate * (1.0 - sig))).astype(BF16)
-    up_b = (act_grad * silu).astype(BF16)
-    thin_ref[:, :wide] = (gate_b[:, :wide].astype(F32) * back_x).astype(BF16)
-    thin_ref[:, wide : 2 * wide] = (up_b[:, :wide].astype(F32) * back_x).astype(BF16)
     for x in range(0, tps // 2, 2):
         at = [pl.ds(pl.multiple_of((2 * (x + i) + c_ref[0]) * share, share), share) for i in range(2)]
-        dx = 0.0
-        for value, refs in ((gate_b, (gate_ref, gate2_ref)), (up_b, (up_ref, up2_ref))):
-            block = [jnp.concatenate([ref[:, a] for a in at], axis=1) for ref in refs]
-            dx = dx + dot(value, jnp.concatenate(block, axis=0))
+        dx = dot(both, jnp.concatenate([in_ref[:, a] for a in at], axis=1))
         for i in range(2):
             out_ref[x + i, :slots, :] = dx[:, i * share : i * share + share].astype(BF16)
             out_ref[x + i, slots:, :] = lines
@@ -208,11 +213,7 @@
     share = width // tps
     c = lax.axis_index("c").astype(jnp.int32)
     tp1 = (lax.axis_index("x").astype(jnp.int32) * cs + c).reshape(1)
-    mine = (
-        jnp.swapaxes(w_gate, 1, 2).reshape(wide, width),
-        jnp.swapaxes(w_up, 1, 2).reshape(wide, width),
-        w_down.reshape(wide, width),
-    )
+    mine = jnp.concatenate([jnp.swapaxes(w_gate, 1, 2), jnp.swapaxes(w_up, 1, 2), w_down]).reshape(3 * wide, width)
     within_t = within_ids.T
 
     sent, target = call(
@@ -226,15 +227,17 @@
         ],
     )
     got = swap(sent.reshape(eps, TILE, 2 * share), "ep")
-    theirs = [lax.ppermute(w, "c", [(0, 1), (1, 0)]) for w in mine]
+    theirs = lax.ppermute(mine, "c", [(0, 1), (1, 0)])
     thin = got[:, :cap, :].reshape(slots, 2 * share).astype(F16)
     full = lax.all_gather(thin, ("x", "c")).astype(BF16)
 
     blocks, thin_b = call(
         experts,
         [shape(xs, slots + 8, share), shape(slots, 3 * wide)],
-        c.reshape(1), full, got.reshape(eps * TILE, 2 * share), *mine, *theirs,
-        smem=1, flops=10**9, scratch=[pltpu.VMEM((slots, width), BF16)] * 2, cap=cap,
+        c.reshape(1), full, got.reshape(eps * TILE, 2 * share), mine, theirs,
+        smem=1, held=(3, 4), flops=10**9, cap=cap,
+        scratch=[pltpu.VMEM((slots, width), BF16)] * 2
+        + [pltpu.VMEM((4 * wide, width), BF16), pltpu.VMEM((2 * wide, width), BF16), pltpu.SemaphoreType.DMA((2, 6))],
     )
     blocks = swap(blocks, "x")
     (home,) = call(gather_up, [shape(eps * TILE, share)], blocks, cap=cap)

time: 114 us -> 113 us (level)
  starting transfers between devices: 35.9 us -> 31.4 us
  waiting for transfers between devices: 14.5 us -> 18.4 us
  local copies, waits for them, and re-layouts: 2.52 us -> 0.07 us
  other arithmetic: 0.5 us -> 1.83 us
    ppermute x3 -> x1, starting transfers between devices: 7.2 us -> 2.85 us  [on_device(): theirs = lax.ppermute(mine, 'c', [(0, 1), (1, 0)])]
    all_to_all x2, waiting for transfers between devices: 14.5 us -> 18.4 us  [swap(): return lax.all_to_all(value, axis, split_axis=0, concat_axis=0, tiled=True)]
    unnamed x14 -> x10, local copies, waits for them, and re-layouts: 2.47 us -> 0.03 us
    concatenate x0 -> x1, other arithmetic: none -> 1.33 us  [on_device(): jnp.concatenate([jnp.swapaxes(w_gate, 1, 2), jnp.swapaxes(w_up, 1, 2), w_...]
  transfers between devices with their start and end apart: 5 -> 3, of which waited for: 2 -> 2; matrix products, arithmetic and copies ran while one was open for 0% -> 2% of each run, Pallas kernels for 2% -> 2%
where the time goes in v3:
time: 113 us; the launch traced here: 112 us
  blocking collectives  49.2 us (44%)
  starting transfers between devices  31.4 us (28%)
  waiting for transfers between devices  18.4 us (16%)
  Pallas kernels  10.6 us (9%)
  other arithmetic  1.83 us (2%)
    all_to_all x2, starting transfers between devices, swap(): return lax.all_to_all(value, axis, split_axis=0, concat_axis=0, tiled=True)  28.5 us
    all_gather x1, blocking collectives, on_device(): full = lax.all_gather(thin, ('x', 'c')).astype(BF16)  26 us
    all_to_all x1, blocking collectives, swap(): return lax.all_to_all(value, axis, split_axis=0, concat_axis=0, tiled=True)  23.1 us
    all_to_all x2, waiting for transfers between devices, swap(): return lax.all_to_all(value, axis, split_axis=0, concat_axis=0, tiled=True)  18.4 us
    pallas_call x5, Pallas kernels, call(): pl.pallas_call(functools.partial(body, **static) if static else body, out...  10.6 us
    ppermute x1, starting transfers between devices, on_device(): theirs = lax.ppermute(mine, 'c', [(0, 1), (1, 0)])  2.85 us
  transfers between devices with their start and end apart: 3, of which 2 were waited for; matrix products, arithmetic and copies ran while one was open for 2% of the time, Pallas kernels for 2%

profile of v3, /device:TPU:1, one launch (start us, length us, event | category | flops | bytes accessed | tf_op | source)
XLA Modules:
  0.0 112.3 jit_solution(15553359320660789412)
XLA Ops:
  0.6 0.0 copy-start.2
  0.6 0.0 copy-start.3
  0.7 0.0 copy-start.4
  0.7 3.0 %route.1 = (bf16[512,256]{1,0:T(8,128)(2,1)}, s32[1,168]{1,0:T(1,128)}) custom-call(s32[1]{0:T(128)} %bitcast.tp_ref, s32[1,168]{1,0:T(1,128)} %bitcast.27, s32[2,168]{1,0:T(2,128)} %bitcast.22, bf16[2,168]{1,0:T(2,128)(2,1)} %bitcast.28, bf16[168,2048]{1,0:T(8,128)(2,1)} %x_hbm.1, bf16[168,2048]{1,0:T(8,128)(2,1)} %dy_hbm.1), custom_call_target="tpu_custom_call" | custom-call | flops 100000000 | bytes 1641760 | tf_op jit(solution)/shard_map/route/pallas_call | solution.py:31
  3.7 24.0 %all-to-all-start = ((bf16[64,8,256]{2,1,0:T(8,128)(2,1)}), bf16[64,8,256]{2,1,0:T(8,128)(2,1)S(1)}, u32[]{:S(2)}, u32[]{:S(2)}) async-start(bf16[64,8,256]{2,1,0:T(8,128)(2,1)} %bitcast.26), calls=%async_computation | async-start | bytes 524288 | tf_op jit(solution)/shard_map/all_to_all | solution.py:18
  27.7 0.0 copy-done.2
  27.7 0.0 copy-done.3
  27.7 0.0 copy-done.4
  27.7 1.3 %pad_maximum_fusion = bf16[6,64,2048]{2,1,0:T(8,128)(2,1)} fusion(bf16[2,64,2048]{2,1,0:T(8,128)(2,1)S(1)} %copy-done.2, bf16[2,64,2048]{2,1,0:T(8,128)(2,1)S(1)} %bitcast.24, bf16[2,64,2048]{2,1,0:T(8,128)(2,1)S(1)} %bitcast.25), kind=kLoop, calls=%fused_computation | loop fusion | flops 1572864 | bytes 3145728 | tf_op jit(solution)/shard_map/concatenate | solution.py:216
  29.0 2.9 %collective-permute-start = (bf16[384,2048]{1,0:T(8,128)(2,1)}, bf16[384,2048]{1,0:T(8,128)(2,1)}, u32[]{:S(2)}, u32[]{:S(2)}) collective-permute-start(bf16[384,2048]{1,0:T(8,128)(2,1)} %bitcast.9.mine_hbm), channel_id=1, source_target_pairs={{0,1},{1,0},{2,3},{3,2},{4,5},{5,4},{6,7},{7,6},{8,9},{9,8},{10,11... | collective-permute-start | bytes 4718600 | tf_op jit(solution)/shard_map/ppermute | solution.py:230
  31.9 8.6 %all-to-all-done = bf16[64,8,256]{2,1,0:T(8,128)(2,1)S(1)} async-done(((bf16[64,8,256]{2,1,0:T(8,128)(2,1)}), bf16[64,8,256]{2,1,0:T(8,128)(2,1)S(1)}, u32[]{:S(2)}, u32[]{:S(2)}) %all-to-all-start) | async-done | bytes 262176 | tf_op jit(solution)/shard_map/all_to_all | solution.py:18
  40.5 0.1 slice_convert_fusion
  40.6 26.0 %all-gather.1 = f16[16,256,256]{2,1,0:T(8,128)(2,1)S(1)} all-gather(f16[1,256,256]{2,1,0:T(8,128)(2,1)S(1)} %convert_element_type.17), channel_id=1, replica_groups=mesh['ep'=64,'x'=8,'c'=2] {'x','c'}, dimensions={0}, use_global_device_ids=true | all-gather | bytes 2228224 | tf_op jit(solution)/shard_map/all_gather | solution.py:232
  66.7 0.4 convert_element_type.18.full_ref
  67.1 0.0 collective-permute-done.theirs_hbm
  67.1 4.0 %experts.1 = (bf16[8,264,128]{2,1,0:T(8,128)(2,1)S(1)}, bf16[256,384]{1,0:T(8,128)(2,1)S(1)}) custom-call(s32[1]{0:T(128)} %bitcast.4.c_ref, bf16[16,256,256]{2,1,0:T(8,128)(2,1)S(1)} %convert_element_type.18.full_ref, bf16[512,256]{1,0:T(8,128)(2,1)S(1)} %bitcast.20, bf16[384,2048]{1,0:T(8,128)(2,1)} %bitcast.9.mine_hbm, ...), custom_call_target="tpu_custom_call" | custom-call | flops 1000000000 | bytes 6242304 | tf_op jit(solution)/shard_map/experts/pallas_call | solution.py:31
  71.1 23.1 %all_to_all.15.blocks_ref = bf16[8,264,128]{2,1,0:T(8,128)(2,1)S(1)} all-to-all(bf16[8,264,128]{2,1,0:T(8,128)(2,1)S(1)} %get-tuple-element.19), channel_id=1, replica_groups=mesh['ep'=64,'x'=8,'c'=2] {'x'}, dimensions={0} | all-to-all | bytes 1081344 | tf_op jit(solution)/shard_map/all_to_all | solution.py:18
  94.3 1.0 gather_up.1
  95.3 4.6 %all-to-all-start.2 = ((bf16[64,8,128]{2,1,0:T(8,128)(2,1)}), bf16[64,8,128]{2,1,0:T(8,128)(2,1)S(1)}, u32[]{:S(2)}, u32[]{:S(2)}) async-start(bf16[64,8,128]{2,1,0:T(8,128)(2,1)} %bitcast.10), calls=%async_computation.2 | async-start | bytes 262144 | tf_op jit(solution)/shard_map/all_to_all | solution.py:18
  99.9 0.0 copy-start
  99.9 0.0 copy-start.1
  99.9 1.7 %weights.1 = (bf16[128,2048]{1,0:T(8,128)(2,1)}, bf16[128,2048]{1,0:T(8,128)(2,1)}, bf16[128,2048]{1,0:T(8,128)(2,1)}) custom-call(bf16[16,256,256]{2,1,0:T(8,128)(2,1)S(1)} %convert_element_type.18.full_ref, bf16[256,384]{1,0:T(8,128)(2,1)S(1)} %get-tuple-element.23.thin_ref), custom_call_target="tpu_custom_call" | custom-call | flops 1000000000 | bytes 3866624 | tf_op jit(solution)/shard_map/weights/pallas_call | solution.py:31
  101.6 9.8 %all-to-all-done.2 = bf16[64,8,128]{2,1,0:T(8,128)(2,1)S(1)} async-done(((bf16[64,8,128]{2,1,0:T(8,128)(2,1)}), bf16[64,8,128]{2,1,0:T(8,128)(2,1)S(1)}, u32[]{:S(2)}, u32[]{:S(2)}) %all-to-all-start.2) | async-done | bytes 131104 | tf_op jit(solution)/shard_map/all_to_all | solution.py:18
  111.4 0.0 copy-done
  111.4 0.0 copy-done.1
  111.4 0.9 settle.1
  (1 shorter events, 0.0 us)
Async XLA Ops:
  0.6 27.0 %copy-start.2 = (bf16[2,64,2048]{2,1,0:T(8,128)(2,1)S(1)}, bf16[2,64,2048]{2,1,0:T(8,128)(2,1)}, u32[]{:S(2)}) copy-start(bf16[2,64,2048]{2,1,0:T(8,128)(2,1)} %param.15) | copy-start | bytes 1572868
  0.6 27.0 %copy-start.3 = (bf16[2,2048,64]{1,2,0:T(8,128)(2,1)S(1)}, bf16[2,2048,64]{1,2,0:T(8,128)(2,1)}, u32[]{:S(2)}) copy-start(bf16[2,2048,64]{1,2,0:T(8,128)(2,1)} %param.14) | copy-start | bytes 1572868
  0.7 27.0 %copy-start.4 = (bf16[2,2048,64]{1,2,0:T(8,128)(2,1)S(1)}, bf16[2,2048,64]{1,2,0:T(8,128)(2,1)}, u32[]{:S(2)}) copy-start(bf16[2,2048,64]{1,2,0:T(8,128)(2,1)} %param.13) | copy-start | bytes 1572868
  3.7 36.8 %all-to-all-start = ((bf16[64,8,256]{2,1,0:T(8,128)(2,1)}), bf16[64,8,256]{2,1,0:T(8,128)(2,1)S(1)}, u32[]{:S(2)}, u32[]{:S(2)}) async-start(bf16[64,8,256]{2,1,0:T(8,128)(2,1)} %bitcast.26), calls=%async_computation | async-start | bytes 524288 | tf_op jit(solution)/shard_map/all_to_all | solution.py:18
  29.0 38.1 %collective-permute-start = (bf16[384,2048]{1,0:T(8,128)(2,1)}, bf16[384,2048]{1,0:T(8,128)(2,1)}, u32[]{:S(2)}, u32[]{:S(2)}) collective-permute-start(bf16[384,2048]{1,0:T(8,128)(2,1)} %bitcast.9.mine_hbm), channel_id=1, source_target_pairs={{0,1},{1,0},{2,3},{3,2},{4,5},{5,4},{6,7},{7,6},{8,9},{9,8},{10,11... | collective-permute-start | bytes 4718600 | tf_op jit(solution)/shard_map/ppermute | solution.py:230
  95.3 16.1 %all-to-all-start.2 = ((bf16[64,8,128]{2,1,0:T(8,128)(2,1)}), bf16[64,8,128]{2,1,0:T(8,128)(2,1)S(1)}, u32[]{:S(2)}, u32[]{:S(2)}) async-start(bf16[64,8,128]{2,1,0:T(8,128)(2,1)} %bitcast.10), calls=%async_computation.2 | async-start | bytes 262144 | tf_op jit(solution)/shard_map/all_to_all | solution.py:18
  99.9 11.5 %copy-start = (s32[168,2]{0,1:T(2,128)S(1)}, s32[168,2]{0,1:T(2,128)}, u32[]{:S(2)}) copy-start(s32[168,2]{0,1:T(2,128)} %param.11) | copy-start | bytes 4036
  99.9 11.5 %copy-start.1 = (s32[1,168]{1,0:T(1,128)S(1)}, s32[1,168]{1,0:T(1,128)}, u32[]{:S(2)}) copy-start(s32[1,168]{1,0:T(1,128)} %get-tuple-element.16.target_ref) | copy-start | bytes 2020

commit v4 on v3

--- a/solution.py
+++ b/solution.py
@@ -121,19 +121,21 @@
             copies.append(
                 pltpu.make_async_copy(hbm.at[pl.ds(piece * j, piece)], ref.at[pl.ds(at, piece)], sems.at[i, j])
             )
-            copies[-1].start()
+    for i in (0, 1, 2, 3, 6, 7, 8, 9, 4, 5, 10, 11):
+        copies[i].start()
     for k in range(tps):
         x_ref[:, k * share : k * share + share] = full_ref[k, :, :share]
         dy_ref[:, k * share : k * share + share] = full_ref[k, :, share:]
-    slot, row = iota((slots, got_ref.shape[0]), 0), iota((slots, got_ref.shape[0]), 1)
-    pick = (row == slot // cap * TILE + cap + slot % cap).astype(BF16)
+    slot = iota((slots, 1), 0)
+    pick = (iota((slots, got_ref.shape[0]), 1) == slot // cap * TILE + cap + slot % cap).astype(BF16)
     side = dot(pick, got_ref[:, :share])
-    for copy in copies:
-        copy.wait()
+    for i in (0, 1, 2, 3, 6, 7, 8, 9):
+        copies[i].wait()
     back_x, back_dy = side[:, 2:3], side[:, 3:4]
-    lane = iota((slots, 2 * wide), 1)
-    weight = jnp.where(lane % wide < wide // 2, side[:, 0:1], side[:, 1:2])
+    weight = jnp.where(iota((1, 2 * wide), 1) % wide < wide // 2, side[:, 0:1], side[:, 1:2])
     pre = dot(x_ref[...], in_ref[...], 1, 1) * back_x
+    for i in (4, 5, 10, 11):
+        copies[i].wait()
     grad = dot(dy_ref[...], down_ref[...], 1, 1) * back_dy
     pre_gate = jnp.concatenate([pre[:, :wide], pre[:, 2 * wide : 3 * wide]], axis=1)
     pre_up = jnp.concatenate([pre[:, wide : 2 * wide], pre[:, 3 * wide :]], axis=1)
@@ -169,7 +171,7 @@
     lines = jnp.concatenate([total[slots : slots + 4], total[slots + 4 :]], axis=1)
     lines = four(lines[0:1] + lines[2:3], lines[1:2] + lines[3:4])
     lines = jnp.concatenate(lines + [jnp.zeros((share - 4, slots), F32)], axis=0).astype(BF16)
-    row, slot = iota((out_ref.shape[0], slots), 0), iota((out_ref.shape[0], slots), 1)
+    row, slot = iota((out_ref.shape[0], slots), 0), iota((1, slots), 1)
     at = slot // cap * TILE + slot % cap
     out = dot((row == at).astype(BF16), dx) + dot((row == at + cap).astype(BF16), lines, 1, 1)
     out_ref[...] = out.astype(BF16)

time: 113 us -> 112 us (level)
  no operation moved by 1% of the time
where the time goes in v4:
time: 112 us
  blocking collectives  49.2 us (44%)
  starting transfers between devices  31.4 us (28%)
  waiting for transfers between devices  18.4 us (16%)
  Pallas kernels  10.5 us (9%)
  other arithmetic  1.83 us (2%)
    all_to_all x2, starting transfers between devices, swap(): return lax.all_to_all(value, axis, split_axis=0, concat_axis=0, tiled=True)  28.5 us
    all_gather x1, blocking collectives, on_device(): full = lax.all_gather(thin, ('x', 'c')).astype(BF16)  26 us
    all_to_all x1, blocking collectives, swap(): return lax.all_to_all(value, axis, split_axis=0, concat_axis=0, tiled=True)  23.1 us
    all_to_all x2, waiting for transfers between devices, swap(): return lax.all_to_all(value, axis, split_axis=0, concat_axis=0, tiled=True)  18.4 us
    pallas_call x5, Pallas kernels, call(): pl.pallas_call(functools.partial(body, **static) if static else body, out...  10.5 us
    ppermute x1, starting transfers between devices, on_device(): theirs = lax.ppermute(mine, 'c', [(0, 1), (1, 0)])  2.85 us
  transfers between devices with their start and end apart: 3, of which 2 were waited for; matrix products, arithmetic and copies ran while one was open for 2% of the time, Pallas kernels for 2%

profile of v4, /device:TPU:1, one launch (start us, length us, event | category | flops | bytes accessed | tf_op | source)
XLA Modules:
  0.0 112.1 jit_solution(9547607362696024771)
XLA Ops:
  0.6 0.0 copy-start.2
  0.6 0.0 copy-start.3
  0.7 0.0 copy-start.4
  0.7 3.0 %route.1 = (bf16[512,256]{1,0:T(8,128)(2,1)}, s32[1,168]{1,0:T(1,128)}) custom-call(s32[1]{0:T(128)} %bitcast.tp_ref, s32[1,168]{1,0:T(1,128)} %bitcast.27, s32[2,168]{1,0:T(2,128)} %bitcast.22, bf16[2,168]{1,0:T(2,128)(2,1)} %bitcast.28, bf16[168,2048]{1,0:T(8,128)(2,1)} %x_hbm.1, bf16[168,2048]{1,0:T(8,128)(2,1)} %dy_hbm.1), custom_call_target="tpu_custom_call" | custom-call | flops 100000000 | bytes 1641760 | tf_op jit(solution)/shard_map/route/pallas_call | solution.py:31
  3.7 24.0 %all-to-all-start = ((bf16[64,8,256]{2,1,0:T(8,128)(2,1)}), bf16[64,8,256]{2,1,0:T(8,128)(2,1)S(1)}, u32[]{:S(2)}, u32[]{:S(2)}) async-start(bf16[64,8,256]{2,1,0:T(8,128)(2,1)} %bitcast.26), calls=%async_computation | async-start | bytes 524288 | tf_op jit(solution)/shard_map/all_to_all | solution.py:18
  27.7 0.0 copy-done.2
  27.7 0.0 copy-done.3
  27.7 0.0 copy-done.4
  27.7 1.3 %pad_maximum_fusion = bf16[6,64,2048]{2,1,0:T(8,128)(2,1)} fusion(bf16[2,64,2048]{2,1,0:T(8,128)(2,1)S(1)} %copy-done.2, bf16[2,64,2048]{2,1,0:T(8,128)(2,1)S(1)} %bitcast.24, bf16[2,64,2048]{2,1,0:T(8,128)(2,1)S(1)} %bitcast.25), kind=kLoop, calls=%fused_computation | loop fusion | flops 1572864 | bytes 3145728 | tf_op jit(solution)/shard_map/concatenate | solution.py:218
  29.0 2.9 %collective-permute-start = (bf16[384,2048]{1,0:T(8,128)(2,1)}, bf16[384,2048]{1,0:T(8,128)(2,1)}, u32[]{:S(2)}, u32[]{:S(2)}) collective-permute-start(bf16[384,2048]{1,0:T(8,128)(2,1)} %bitcast.9.mine_hbm), channel_id=1, source_target_pairs={{0,1},{1,0},{2,3},{3,2},{4,5},{5,4},{6,7},{7,6},{8,9},{9,8},{10,11... | collective-permute-start | bytes 4718600 | tf_op jit(solution)/shard_map/ppermute | solution.py:232
  31.9 8.6 %all-to-all-done = bf16[64,8,256]{2,1,0:T(8,128)(2,1)S(1)} async-done(((bf16[64,8,256]{2,1,0:T(8,128)(2,1)}), bf16[64,8,256]{2,1,0:T(8,128)(2,1)S(1)}, u32[]{:S(2)}, u32[]{:S(2)}) %all-to-all-start) | async-done | bytes 262176 | tf_op jit(solution)/shard_map/all_to_all | solution.py:18
  40.5 0.1 slice_convert_fusion
  40.6 26.0 %all-gather.1 = f16[16,256,256]{2,1,0:T(8,128)(2,1)S(1)} all-gather(f16[1,256,256]{2,1,0:T(8,128)(2,1)S(1)} %convert_element_type.17), channel_id=1, replica_groups=mesh['ep'=64,'x'=8,'c'=2] {'x','c'}, dimensions={0}, use_global_device_ids=true | all-gather | bytes 2228224 | tf_op jit(solution)/shard_map/all_gather | solution.py:234
  66.7 0.4 convert_element_type.18.full_ref
  67.1 0.0 collective-permute-done.theirs_hbm
  67.1 3.9 %experts.1 = (bf16[8,264,128]{2,1,0:T(8,128)(2,1)S(1)}, bf16[256,384]{1,0:T(8,128)(2,1)S(1)}) custom-call(s32[1]{0:T(128)} %bitcast.4.c_ref, bf16[16,256,256]{2,1,0:T(8,128)(2,1)S(1)} %convert_element_type.18.full_ref, bf16[512,256]{1,0:T(8,128)(2,1)S(1)} %bitcast.20, bf16[384,2048]{1,0:T(8,128)(2,1)} %bitcast.9.mine_hbm, ...), custom_call_target="tpu_custom_call" | custom-call | flops 1000000000 | bytes 6242304 | tf_op jit(solution)/shard_map/experts/pallas_call | solution.py:31
  71.0 23.1 %all_to_all.15.blocks_ref = bf16[8,264,128]{2,1,0:T(8,128)(2,1)S(1)} all-to-all(bf16[8,264,128]{2,1,0:T(8,128)(2,1)S(1)} %get-tuple-element.19), channel_id=1, replica_groups=mesh['ep'=64,'x'=8,'c'=2] {'x'}, dimensions={0} | all-to-all | bytes 1081344 | tf_op jit(solution)/shard_map/all_to_all | solution.py:18
  94.1 1.0 gather_up.1
  95.1 4.6 %all-to-all-start.2 = ((bf16[64,8,128]{2,1,0:T(8,128)(2,1)}), bf16[64,8,128]{2,1,0:T(8,128)(2,1)S(1)}, u32[]{:S(2)}, u32[]{:S(2)}) async-start(bf16[64,8,128]{2,1,0:T(8,128)(2,1)} %bitcast.10), calls=%async_computation.2 | async-start | bytes 262144 | tf_op jit(solution)/shard_map/all_to_all | solution.py:18
  99.7 0.0 copy-start
  99.7 0.0 copy-start.1
  99.7 1.7 %weights.1 = (bf16[128,2048]{1,0:T(8,128)(2,1)}, bf16[128,2048]{1,0:T(8,128)(2,1)}, bf16[128,2048]{1,0:T(8,128)(2,1)}) custom-call(bf16[16,256,256]{2,1,0:T(8,128)(2,1)S(1)} %convert_element_type.18.full_ref, bf16[256,384]{1,0:T(8,128)(2,1)S(1)} %get-tuple-element.23.thin_ref), custom_call_target="tpu_custom_call" | custom-call | flops 1000000000 | bytes 3866624 | tf_op jit(solution)/shard_map/weights/pallas_call | solution.py:31
  101.5 9.8 %all-to-all-done.2 = bf16[64,8,128]{2,1,0:T(8,128)(2,1)S(1)} async-done(((bf16[64,8,128]{2,1,0:T(8,128)(2,1)}), bf16[64,8,128]{2,1,0:T(8,128)(2,1)S(1)}, u32[]{:S(2)}, u32[]{:S(2)}) %all-to-all-start.2) | async-done | bytes 131104 | tf_op jit(solution)/shard_map/all_to_all | solution.py:18
  111.3 0.0 copy-done
  111.3 0.0 copy-done.1
  111.3 0.9 settle.1
  (1 shorter events, 0.0 us)
Async XLA Ops:
  0.6 27.0 %copy-start.2 = (bf16[2,64,2048]{2,1,0:T(8,128)(2,1)S(1)}, bf16[2,64,2048]{2,1,0:T(8,128)(2,1)}, u32[]{:S(2)}) copy-start(bf16[2,64,2048]{2,1,0:T(8,128)(2,1)} %param.15) | copy-start | bytes 1572868
  0.6 27.0 %copy-start.3 = (bf16[2,2048,64]{1,2,0:T(8,128)(2,1)S(1)}, bf16[2,2048,64]{1,2,0:T(8,128)(2,1)}, u32[]{:S(2)}) copy-start(bf16[2,2048,64]{1,2,0:T(8,128)(2,1)} %param.14) | copy-start | bytes 1572868
  0.7 27.0 %copy-start.4 = (bf16[2,2048,64]{1,2,0:T(8,128)(2,1)S(1)}, bf16[2,2048,64]{1,2,0:T(8,128)(2,1)}, u32[]{:S(2)}) copy-start(bf16[2,2048,64]{1,2,0:T(8,128)(2,1)} %param.13) | copy-start | bytes 1572868
  3.7 36.8 %all-to-all-start = ((bf16[64,8,256]{2,1,0:T(8,128)(2,1)}), bf16[64,8,256]{2,1,0:T(8,128)(2,1)S(1)}, u32[]{:S(2)}, u32[]{:S(2)}) async-start(bf16[64,8,256]{2,1,0:T(8,128)(2,1)} %bitcast.26), calls=%async_computation | async-start | bytes 524288 | tf_op jit(solution)/shard_map/all_to_all | solution.py:18
  29.0 38.1 %collective-permute-start = (bf16[384,2048]{1,0:T(8,128)(2,1)}, bf16[384,2048]{1,0:T(8,128)(2,1)}, u32[]{:S(2)}, u32[]{:S(2)}) collective-permute-start(bf16[384,2048]{1,0:T(8,128)(2,1)} %bitcast.9.mine_hbm), channel_id=1, source_target_pairs={{0,1},{1,0},{2,3},{3,2},{4,5},{5,4},{6,7},{7,6},{8,9},{9,8},{10,11... | collective-permute-start | bytes 4718600 | tf_op jit(solution)/shard_map/ppermute | solution.py:232
  95.1 16.1 %all-to-all-start.2 = ((bf16[64,8,128]{2,1,0:T(8,128)(2,1)}), bf16[64,8,128]{2,1,0:T(8,128)(2,1)S(1)}, u32[]{:S(2)}, u32[]{:S(2)}) async-start(bf16[64,8,128]{2,1,0:T(8,128)(2,1)} %bitcast.10), calls=%async_computation.2 | async-start | bytes 262144 | tf_op jit(solution)/shard_map/all_to_all | solution.py:18
  99.7 11.5 %copy-start = (s32[168,2]{0,1:T(2,128)S(1)}, s32[168,2]{0,1:T(2,128)}, u32[]{:S(2)}) copy-start(s32[168,2]{0,1:T(2,128)} %param.11) | copy-start | bytes 4036
  99.7 11.5 %copy-start.1 = (s32[1,168]{1,0:T(1,128)S(1)}, s32[1,168]{1,0:T(1,128)}, u32[]{:S(2)}) copy-start(s32[1,168]{1,0:T(1,128)} %get-tuple-element.16.target_ref) | copy-start | bytes 2020

commit v5 on v4

--- a/solution.py
+++ b/solution.py
@@ -86,12 +86,13 @@
     lane = iota((rows, share), 1)
     for copy in copies[3:]:
         copy.wait()
-    parts, side = [], 0.0
-    for i, ref in enumerate((x_ref, dy_ref)):
-        top = jnp.max(jnp.abs(ref[...]), axis=1, keepdims=True).astype(F32)
-        up, down = power(jnp.maximum(top, 2.0**-100))
-        parts.append((ref[:, pl.ds(at, share)].astype(F32) * up).astype(BF16))
-        side = side + jnp.where(lane == 2 + i, down, 0.0)
+    tops = [jnp.max(jnp.abs(ref[...]), axis=1, keepdims=True).astype(F32) for ref in (x_ref, dy_ref)]
+    up, down = power(jnp.maximum(jnp.where(lane == 2, tops[0], tops[1]), 2.0**-100))
+    side = jnp.where((lane == 2) | (lane == 3), down, 0.0)
+    parts = [
+        (ref[:, pl.ds(at, share)].astype(F32) * up[:, 2 + i : 3 + i]).astype(BF16)
+        for i, ref in enumerate((x_ref, dy_ref))
+    ]
     sides = sides + dot(beside, side.astype(BF16))
     sent_ref[:, :share] = (dot(place, parts[0]) + sides).astype(BF16)
     sent_ref[:, share:] = dot(place, parts[1]).astype(BF16)

time: 112 us -> 112 us (level)
  no operation moved by 1% of the time
where the time goes in v5:
time: 112 us
  blocking collectives  49.2 us (44%)
  starting transfers between devices  31.4 us (28%)
  waiting for transfers between devices  18.4 us (16%)
  Pallas kernels  10.4 us (9%)
  other arithmetic  1.83 us (2%)
    all_to_all x2, starting transfers between devices, swap(): return lax.all_to_all(value, axis, split_axis=0, concat_axis=0, tiled=True)  28.5 us
    all_gather x1, blocking collectives, on_device(): full = lax.all_gather(thin, ('x', 'c')).astype(BF16)  26 us
    all_to_all x1, blocking collectives, swap(): return lax.all_to_all(value, axis, split_axis=0, concat_axis=0, tiled=True)  23.2 us
    all_to_all x2, waiting for transfers between devices, swap(): return lax.all_to_all(value, axis, split_axis=0, concat_axis=0, tiled=True)  18.4 us
    pallas_call x5, Pallas kernels, call(): pl.pallas_call(functools.partial(body, **static) if static else body, out...  10.4 us
    ppermute x1, starting transfers between devices, on_device(): theirs = lax.ppermute(mine, 'c', [(0, 1), (1, 0)])  2.85 us
  transfers between devices with their start and end apart: 3, of which 2 were waited for; matrix products, arithmetic and copies ran while one was open for 2% of the time, Pallas kernels for 2%

profile of v5, /device:TPU:1, one launch (start us, length us, event | category | flops | bytes accessed | tf_op | source)
XLA Modules:
  0.0 112.0 jit_solution(3868739951654925970)
XLA Ops:
  0.6 0.0 copy-start.2
  0.6 0.0 copy-start.3
  0.7 0.0 copy-start.4
  0.7 2.9 %route.1 = (bf16[512,256]{1,0:T(8,128)(2,1)}, s32[1,168]{1,0:T(1,128)}) custom-call(s32[1]{0:T(128)} %bitcast.tp_ref, s32[1,168]{1,0:T(1,128)} %bitcast.27, s32[2,168]{1,0:T(2,128)} %bitcast.22, bf16[2,168]{1,0:T(2,128)(2,1)} %bitcast.28, bf16[168,2048]{1,0:T(8,128)(2,1)} %x_hbm.1, bf16[168,2048]{1,0:T(8,128)(2,1)} %dy_hbm.1), custom_call_target="tpu_custom_call" | custom-call | flops 100000000 | bytes 1641760 | tf_op jit(solution)/shard_map/route/pallas_call | solution.py:31
  3.6 24.0 %all-to-all-start = ((bf16[64,8,256]{2,1,0:T(8,128)(2,1)}), bf16[64,8,256]{2,1,0:T(8,128)(2,1)S(1)}, u32[]{:S(2)}, u32[]{:S(2)}) async-start(bf16[64,8,256]{2,1,0:T(8,128)(2,1)} %bitcast.26), calls=%async_computation | async-start | bytes 524288 | tf_op jit(solution)/shard_map/all_to_all | solution.py:18
  27.6 0.0 copy-done.2
  27.6 0.0 copy-done.3
  27.6 0.0 copy-done.4
  27.6 1.3 %pad_maximum_fusion = bf16[6,64,2048]{2,1,0:T(8,128)(2,1)} fusion(bf16[2,64,2048]{2,1,0:T(8,128)(2,1)S(1)} %copy-done.2, bf16[2,64,2048]{2,1,0:T(8,128)(2,1)S(1)} %bitcast.24, bf16[2,64,2048]{2,1,0:T(8,128)(2,1)S(1)} %bitcast.25), kind=kLoop, calls=%fused_computation | loop fusion | flops 1572864 | bytes 3145728 | tf_op jit(solution)/shard_map/concatenate | solution.py:219
  28.9 2.9 %collective-permute-start = (bf16[384,2048]{1,0:T(8,128)(2,1)}, bf16[384,2048]{1,0:T(8,128)(2,1)}, u32[]{:S(2)}, u32[]{:S(2)}) collective-permute-start(bf16[384,2048]{1,0:T(8,128)(2,1)} %bitcast.9.mine_hbm), channel_id=1, source_target_pairs={{0,1},{1,0},{2,3},{3,2},{4,5},{5,4},{6,7},{7,6},{8,9},{9,8},{10,11... | collective-permute-start | bytes 4718600 | tf_op jit(solution)/shard_map/ppermute | solution.py:233
  31.8 8.6 %all-to-all-done = bf16[64,8,256]{2,1,0:T(8,128)(2,1)S(1)} async-done(((bf16[64,8,256]{2,1,0:T(8,128)(2,1)}), bf16[64,8,256]{2,1,0:T(8,128)(2,1)S(1)}, u32[]{:S(2)}, u32[]{:S(2)}) %all-to-all-start) | async-done | bytes 262176 | tf_op jit(solution)/shard_map/all_to_all | solution.py:18
  40.4 0.1 slice_convert_fusion
  40.5 26.0 %all-gather.1 = f16[16,256,256]{2,1,0:T(8,128)(2,1)S(1)} all-gather(f16[1,256,256]{2,1,0:T(8,128)(2,1)S(1)} %convert_element_type.17), channel_id=1, replica_groups=mesh['ep'=64,'x'=8,'c'=2] {'x','c'}, dimensions={0}, use_global_device_ids=true | all-gather | bytes 2228224 | tf_op jit(solution)/shard_map/all_gather | solution.py:235
  66.5 0.4 convert_element_type.18.full_ref
  67.0 0.0 collective-permute-done.theirs_hbm
  67.0 3.9 %experts.1 = (bf16[8,264,128]{2,1,0:T(8,128)(2,1)S(1)}, bf16[256,384]{1,0:T(8,128)(2,1)S(1)}) custom-call(s32[1]{0:T(128)} %bitcast.4.c_ref, bf16[16,256,256]{2,1,0:T(8,128)(2,1)S(1)} %convert_element_type.18.full_ref, bf16[512,256]{1,0:T(8,128)(2,1)S(1)} %bitcast.20, bf16[384,2048]{1,0:T(8,128)(2,1)} %bitcast.9.mine_hbm, ...), custom_call_target="tpu_custom_call" | custom-call | flops 1000000000 | bytes 6242304 | tf_op jit(solution)/shard_map/experts/pallas_call | solution.py:31
  70.9 23.2 %all_to_all.15.blocks_ref = bf16[8,264,128]{2,1,0:T(8,128)(2,1)S(1)} all-to-all(bf16[8,264,128]{2,1,0:T(8,128)(2,1)S(1)} %get-tuple-element.19), channel_id=1, replica_groups=mesh['ep'=64,'x'=8,'c'=2] {'x'}, dimensions={0} | all-to-all | bytes 1081344 | tf_op jit(solution)/shard_map/all_to_all | solution.py:18
  94.0 1.0 gather_up.1
  95.0 4.6 %all-to-all-start.2 = ((bf16[64,8,128]{2,1,0:T(8,128)(2,1)}), bf16[64,8,128]{2,1,0:T(8,128)(2,1)S(1)}, u32[]{:S(2)}, u32[]{:S(2)}) async-start(bf16[64,8,128]{2,1,0:T(8,128)(2,1)} %bitcast.10), calls=%async_computation.2 | async-start | bytes 262144 | tf_op jit(solution)/shard_map/all_to_all | solution.py:18
  99.6 0.0 copy-start
  99.6 0.0 copy-start.1
  99.6 1.7 %weights.1 = (bf16[128,2048]{1,0:T(8,128)(2,1)}, bf16[128,2048]{1,0:T(8,128)(2,1)}, bf16[128,2048]{1,0:T(8,128)(2,1)}) custom-call(bf16[16,256,256]{2,1,0:T(8,128)(2,1)S(1)} %convert_element_type.18.full_ref, bf16[256,384]{1,0:T(8,128)(2,1)S(1)} %get-tuple-element.23.thin_ref), custom_call_target="tpu_custom_call" | custom-call | flops 1000000000 | bytes 3866624 | tf_op jit(solution)/shard_map/weights/pallas_call | solution.py:31
  101.4 9.8 %all-to-all-done.2 = bf16[64,8,128]{2,1,0:T(8,128)(2,1)S(1)} async-done(((bf16[64,8,128]{2,1,0:T(8,128)(2,1)}), bf16[64,8,128]{2,1,0:T(8,128)(2,1)S(1)}, u32[]{:S(2)}, u32[]{:S(2)}) %all-to-all-start.2) | async-done | bytes 131104 | tf_op jit(solution)/shard_map/all_to_all | solution.py:18
  111.2 0.0 copy-done
  111.2 0.0 copy-done.1
  111.2 0.9 settle.1
  (1 shorter events, 0.0 us)
Async XLA Ops:
  0.6 26.9 %copy-start.2 = (bf16[2,64,2048]{2,1,0:T(8,128)(2,1)S(1)}, bf16[2,64,2048]{2,1,0:T(8,128)(2,1)}, u32[]{:S(2)}) copy-start(bf16[2,64,2048]{2,1,0:T(8,128)(2,1)} %param.15) | copy-start | bytes 1572868
  0.6 26.9 %copy-start.3 = (bf16[2,2048,64]{1,2,0:T(8,128)(2,1)S(1)}, bf16[2,2048,64]{1,2,0:T(8,128)(2,1)}, u32[]{:S(2)}) copy-start(bf16[2,2048,64]{1,2,0:T(8,128)(2,1)} %param.14) | copy-start | bytes 1572868
  0.7 26.9 %copy-start.4 = (bf16[2,2048,64]{1,2,0:T(8,128)(2,1)S(1)}, bf16[2,2048,64]{1,2,0:T(8,128)(2,1)}, u32[]{:S(2)}) copy-start(bf16[2,2048,64]{1,2,0:T(8,128)(2,1)} %param.13) | copy-start | bytes 1572868
  3.6 36.8 %all-to-all-start = ((bf16[64,8,256]{2,1,0:T(8,128)(2,1)}), bf16[64,8,256]{2,1,0:T(8,128)(2,1)S(1)}, u32[]{:S(2)}, u32[]{:S(2)}) async-start(bf16[64,8,256]{2,1,0:T(8,128)(2,1)} %bitcast.26), calls=%async_computation | async-start | bytes 524288 | tf_op jit(solution)/shard_map/all_to_all | solution.py:18
  28.9 38.1 %collective-permute-start = (bf16[384,2048]{1,0:T(8,128)(2,1)}, bf16[384,2048]{1,0:T(8,128)(2,1)}, u32[]{:S(2)}, u32[]{:S(2)}) collective-permute-start(bf16[384,2048]{1,0:T(8,128)(2,1)} %bitcast.9.mine_hbm), channel_id=1, source_target_pairs={{0,1},{1,0},{2,3},{3,2},{4,5},{5,4},{6,7},{7,6},{8,9},{9,8},{10,11... | collective-permute-start | bytes 4718600 | tf_op jit(solution)/shard_map/ppermute | solution.py:233
  95.0 16.1 %all-to-all-start.2 = ((bf16[64,8,128]{2,1,0:T(8,128)(2,1)}), bf16[64,8,128]{2,1,0:T(8,128)(2,1)S(1)}, u32[]{:S(2)}, u32[]{:S(2)}) async-start(bf16[64,8,128]{2,1,0:T(8,128)(2,1)} %bitcast.10), calls=%async_computation.2 | async-start | bytes 262144 | tf_op jit(solution)/shard_map/all_to_all | solution.py:18
  99.6 11.5 %copy-start = (s32[168,2]{0,1:T(2,128)S(1)}, s32[168,2]{0,1:T(2,128)}, u32[]{:S(2)}) copy-start(s32[168,2]{0,1:T(2,128)} %param.11) | copy-start | bytes 4036
  99.6 11.5 %copy-start.1 = (s32[1,168]{1,0:T(1,128)S(1)}, s32[1,168]{1,0:T(1,128)}, u32[]{:S(2)}) copy-start(s32[1,168]{1,0:T(1,128)} %get-tuple-element.16.target_ref) | copy-start | bytes 2020
